TPU v7x, 128 devices: a whole 4x4x4 slice. The times are simulated.
128 devices in a mesh: sp: 16 (over z, y), dp: 8 (over x, core).
Axes of the slice: x: 4, y: 4, z: 4, core: 2. Of those that a mesh axis runs over, the one named last changes fastest.
Arguments:
- queries: bfloat16 [8, 2048, 2048], P('dp', 'sp'), may hold values from -8 to 8
- keys: bfloat16 [8, 2048, 2048], P('dp', 'sp'), may hold values from -8 to 8
- values: bfloat16 [8, 2048, 2048], P('dp', 'sp'), may hold values from -6 to 6
- proj_weight: bfloat16 [2048, 2048], P('sp'), may hold values from -0.125 to 0.125
- residual: bfloat16 [8, 2048, 2048], P('dp', 'sp'), may hold values from -6 to 6
- norm_gain: float32 [2048], replicated, may hold values from 0.1 to 1.9
- route: int32 [8, 2048, 2], P('dp', 'sp'), may hold values from 0 to 15, all different within a row; in each aligned block of 128 rows (0 to 127, 128 to 255, ..., all dimensions but the last counted through in order) at most 32 rows name the same one
- route_weight: float32 [8, 2048, 2], P('dp', 'sp'), may hold values from 0.1 to 1
- w_gate: bfloat16 [16, 2048, 1024], P('sp'), may hold values from -0.125 to 0.125
- w_up: bfloat16 [16, 2048, 1024], P('sp'), may hold values from -0.125 to 0.125
- w_down: bfloat16 [16, 1024, 2048], P('sp'), may hold values from -0.1875 to 0.1875
Outputs:
- mixed: bfloat16 [8, 2048, 2048], P('dp', 'sp')
Inputs may be any that keep to these rules, and one draw needn't show every extreme that they name: `route`: in the rows of one device no expert is named by more than 32 rows, a bound that some block reaches.
All inputs are finite; a program needn't handle non-finite values.
Results may differ from a plain program's by a relative error of at most 0.013.
Values may be sent and summed in bfloat16 or wider, within the bound.
A program may use at most 128 MiB of HBM per device.

v0:
```python
import jax
import jax.numpy as jnp
from jax import lax
from jax.sharding import PartitionSpec as P

HEADS = 16


EPS = 1e-06


def sent_together(arrays, axis, split_dim, concat_dim, along):
    both = jnp.concatenate(arrays, axis=along)
    out, at, finished = (
        lax.all_to_all(both, axis, split_axis=split_dim, concat_axis=concat_dim, tiled=True),
        0,
        [],
    )
    for a in arrays:
        finished.append(lax.slice_in_dim(out, at, at + a.shape[along], axis=along))
        at += a.shape[along]
    return tuple(finished)


def stick_breaking(query, key, value, heads_here):
    length, width = query.shape
    head_size = width // heads_here
    query_heads = query.reshape(length, heads_here, head_size)
    key_heads = key.reshape(length, heads_here, head_size)
    value_heads = value.reshape(length, heads_here, head_size)
    block = min(512, length)
    blocks = length // block
    groups = min(4, blocks)
    results = []
    for group in range(groups):
        first = group * blocks // groups
        last = (group + 1) * blocks // groups
        key_len = last * block
        near_keys = key_heads[:key_len]
        near_values = value_heads[:key_len]
        starts = jnp.arange(first, last, dtype=jnp.int32) * block
        query_blocks = query_heads[first * block : last * block].reshape(
            last - first, block, heads_here, head_size
        )

        def one_block(args):
            query_block, start = args
            scores = jnp.einsum(
                "qhd,khd->hqk", query_block, near_keys, preferred_element_type=jnp.float32
            ) * head_size ** (-0.5)
            query_pos = start + jnp.arange(block)
            causal = jnp.arange(key_len)[None, :] < query_pos[:, None]
            softer = jnp.where(causal, jax.nn.softplus(scores), 0.0)
            suffix = lax.cumsum(softer, axis=2, reverse=True)
            weight = jnp.exp(jnp.where(causal, scores - suffix, -jnp.inf)).astype(jnp.bfloat16)
            attended = jnp.einsum(
                "hqk,khd->qhd", weight, near_values, preferred_element_type=jnp.float32
            )
            return attended.astype(jnp.bfloat16).reshape(block, heads_here * head_size)

        results.append(
            lax.map(one_block, (query_blocks, starts)).reshape((last - first) * block, width)
        )
    return jnp.concatenate(results, axis=0)


def body(
    queries,
    keys,
    values,
    proj_weight,
    residual,
    norm_gain,
    route,
    route_weight,
    w_gate,
    w_up,
    w_down,
):
    seq_span = lax.axis_size("sp")
    rows = queries.shape[1]
    width = queries.shape[2]
    heads_here = HEADS // seq_span
    query_all, key_all, value_all = sent_together((queries, keys, values), "sp", 2, 1, 0)
    attended = stick_breaking(query_all[0], key_all[0], value_all[0], heads_here)
    gathered = lax.all_to_all(attended[None], "sp", split_axis=1, concat_axis=2, tiled=True)[0]
    projected = jnp.dot(
        gathered,
        lax.all_gather(proj_weight, "sp", axis=0, tiled=True),
        preferred_element_type=jnp.float32,
    )
    stream = (residual[0].astype(jnp.float32) + projected).astype(jnp.bfloat16)
    stream_f = stream.astype(jnp.float32)
    normed = (
        stream_f
        * lax.rsqrt(jnp.mean(stream_f * stream_f, axis=-1, keepdims=True) + EPS)
        * norm_gain
    ).astype(jnp.bfloat16)
    capacity = 4 * rows // seq_span
    chosen = route[0].reshape(rows * 2)
    one_hot = (chosen[:, None] == jnp.arange(seq_span, dtype=jnp.int32)[None, :]).astype(jnp.int32)
    earlier = jnp.cumsum(one_hot, axis=0) - one_hot
    slot = jnp.sum(earlier * one_hot, axis=1)
    target = chosen * capacity + slot
    source_row = jnp.arange(rows * 2, dtype=jnp.int32) // 2
    slot_source = jnp.zeros((seq_span * capacity,), jnp.int32).at[target].set(source_row)
    slot_used = jnp.zeros((seq_span * capacity,), jnp.bool_).at[target].set(True)
    outgoing = jnp.where(slot_used[:, None], normed[slot_source], jnp.zeros((), jnp.bfloat16))
    outgoing = outgoing.reshape(seq_span, capacity, width)
    arrived = lax.all_to_all(outgoing, "sp", split_axis=0, concat_axis=0, tiled=True)
    senders, slots, features = arrived.shape
    flat = arrived.reshape(senders * slots, features)
    gate = jnp.dot(flat, w_gate[0], preferred_element_type=jnp.float32)
    upper = jnp.dot(flat, w_up[0], preferred_element_type=jnp.float32)
    hidden = (jax.nn.silu(gate) * upper).astype(jnp.bfloat16)
    result = jnp.dot(hidden, w_down[0], preferred_element_type=jnp.float32).astype(jnp.bfloat16)
    returned = lax.all_to_all(
        result.reshape(senders, slots, features), "sp", split_axis=0, concat_axis=0, tiled=True
    )
    picked = returned.reshape(seq_span * capacity, width)[target].reshape(rows, 2, width)
    mixed = stream_f + jnp.sum(route_weight[0][:, :, None] * picked.astype(jnp.float32), axis=1)
    return mixed.astype(jnp.bfloat16)[None]


def solution(mesh):
    return jax.shard_map(
        body,
        mesh=mesh,
        in_specs=(
            P("dp", "sp", None),
            P("dp", "sp", None),
            P("dp", "sp", None),
            P("sp", None),
            P("dp", "sp", None),
            P(),
            P("dp", "sp", None),
            P("dp", "sp", None),
            P("sp", None, None),
            P("sp", None, None),
            P("sp", None, None),
        ),
        out_specs=P("dp", "sp", None),
        check_vma=False,
    )
```

profile of v0, /device:TPU:0, one launch (start us, length us, event | category | flops | bytes accessed | tf_op | source)
XLA Modules:
  0.0 325.2 jit_solution(16853251736767555730)
XLA Ops:
  14.3 4.5 %pad_maximum_fusion = bf16[3,128,2048]{1,0,2:T(4,128)(2,1)} fusion(bf16[1,128,2048]{1,0,2:T(2,128)(2,1)S(1)} %copy.114, bf16[1,128,2048]{1,0,2:T(2,128)(2,1)S(1)} %copy.113, bf16[1,128,2048]{1,0,2:T(2,128)(2,1)S(1)} %copy.112), kind=kLoop, calls=%fused_computation.39 | loop fusion | flops 4718592 | bytes 3145728 | tf_op jit(solution)/shard_map/concatenate | solution.py:13
  18.9 8.5 %all-to-all-start = ((bf16[3,128,2048]{1,0,2:T(4,128)(2,1)}), bf16[3,128,2048]{1,0,2:T(4,128)(2,1)}, u32[]{:S(2)}, u32[]{:S(2)}) async-start(bf16[3,128,2048]{1,0,2:T(4,128)(2,1)} %pad_maximum_fusion), calls=%async_computation | async-start | bytes 4194304 | tf_op jit(solution)/shard_map/all_to_all | solution.py:15
  31.2 34.0 %all-to-all-done = bf16[3,128,2048]{1,0,2:T(4,128)(2,1)} async-done(((bf16[3,128,2048]{1,0,2:T(4,128)(2,1)}), bf16[3,128,2048]{1,0,2:T(4,128)(2,1)}, u32[]{:S(2)}, u32[]{:S(2)}) %all-to-all-start) | async-done | bytes 1572896 | tf_op jit(solution)/shard_map/all_to_all | solution.py:15
  65.2 2.4 copy.115
  70.5 4.8 %fusion.46 = f32[1,512,4,128]{1,2,3,0:T(4,128)S(1)} fusion(f32[1,512,4,128]{1,3,2,0:T(8,128)S(1)} %bitcast.221), kind=kOutput, calls=%fused_computation.61 | output fusion | flops 33292288 | bytes 2097152 | tf_op jit(solution)/shard_map/reduce-window
  78.5 6.3 %fusion.14 = (f32[512,1536]{1,0:T(8,128)}, f32[512,1536]{1,0:T(8,128)}) fusion(s32[512]{0:T(512)S(1)} %iota_add_fusion.1, bf16[512,128]{1,0:T(8,128)(2,1)S(1)} %bitcast.226, bf16[1536,128]{1,0:T(8,128)(2,1)} %bitcast.225), kind=kOutput, calls=%fused_computation.24 | convolution fusion | flops 208404480 | bytes 6817792 | tf_op jit(solution)/shard_map/while/body/eval_jaxpr/qhd,khd->hqk/dot_general | solution.py:48
  84.8 4.1 %copy.130 = f32[512,1536]{0,1:T(8,128)} copy(f32[512,1536]{1,0:T(8,128)} %get-tuple-element.70) | data formatting | bytes 6291456 | tf_op jit(solution)/shard_map/while/body/eval_jaxpr/jit(_where)/select_n | solution.py:53
  88.9 11.9 %fusion.12 = f32[1,512,12,128]{1,2,3,0:T(8,128)S(1)} fusion(f32[1,512,12,128]{1,3,2,0:T(8,128)} %bitcast.203), kind=kOutput, calls=%fused_computation.20 | output fusion | flops 99876864 | bytes 6291456 | tf_op jit(solution)/shard_map/reduce-window.4
  100.8 3.7 %copy.132 = f32[1,512,12,128]{1,3,2,0:T(8,128)} copy(f32[1,512,12,128]{1,2,3,0:T(8,128)S(1)} %fusion.12) | data formatting | bytes 6291456 | tf_op jit(solution)/shard_map/reduce-window.4
  107.5 3.6 %copy.134 = f32[512,1536]{1,0:T(8,128)} copy(f32[512,1536]{0,1:T(8,128)} %bitcast.204) | data formatting | bytes 6291456 | tf_op jit(solution)/shard_map/reshape.176
  111.1 3.7 %copy.133 = f32[512,1536]{1,0:T(8,128)} copy(f32[512,1536]{0,1:T(8,128)} %bitcast.202) | data formatting | bytes 6291456 | tf_op jit(solution)/shard_map/reshape.175
  119.8 3.2 copy.124
  122.9 7.2 %fusion.70 = f32[1,512,8,128]{1,2,3,0:T(8,128)} fusion(f32[1,512,8,128]{1,2,3,0:T(8,128)} %copy.124), kind=kOutput, calls=%fused_computation.113 | output fusion | flops 66584576 | bytes 4194304 | tf_op jit(solution)/shard_map/reduce-window.2
  130.1 3.1 copy.125
  140.5 3.0 fusion.1
  143.6 2.8 copy.153
  146.4 6.0 %copy.138 = f32[1,512,16,128]{1,2,3,0:T(8,128)} copy(f32[1,512,16,128]{3,2,1,0:T(8,128)} %bitcast.197) | data formatting | bytes 8388608 | tf_op jit(solution)/shard_map/reshape.17
  152.4 12.7 %fusion.71 = f32[1,512,16,128]{1,2,3,0:T(8,128)} fusion(f32[1,512,16,128]{1,2,3,0:T(8,128)} %copy.138), kind=kOutput, calls=%fused_computation.114 | output fusion | flops 133169152 | bytes 8388608 | tf_op jit(solution)/shard_map/reduce-window.6
  165.1 6.1 %copy.139 = f32[1,512,16,128]{3,2,1,0:T(8,128)} copy(f32[1,512,16,128]{1,2,3,0:T(8,128)} %fusion.71) | data formatting | bytes 8388608 | tf_op jit(solution)/shard_map/reduce-window.6
  189.4 3.2 fusion.38
  194.0 11.5 %reduce.2 = bf16[2048,128]{1,0:T(8,128)(2,1)S(1)} reduce(bf16[2048,1,128]{2,1,0:T(2,128)(2,1)S(1)} %bitcast.210, bf16[]{:T(256)} %broadcast.192), dimensions={1}, to_apply=%bitcast.172.reduce_sub_computation | reduce | bytes 1048578
  206.4 3.6 %all-to-all-start.1 = ((bf16[16,2,8192]{2,1,0:T(2,128)(2,1)}), bf16[16,2,8192]{2,1,0:T(2,128)(2,1)S(1)}, u32[]{:S(2)}, u32[]{:S(2)}) async-start(bf16[16,2,8192]{2,1,0:T(2,128)(2,1)} %reshape.431), calls=%async_computation.1 | async-start | bytes 1048576 | tf_op jit(solution)/shard_map/all_to_all | solution.py:86
  213.3 7.8 %all-to-all-done.1 = bf16[16,2,8192]{2,1,0:T(2,128)(2,1)S(1)} async-done(((bf16[16,2,8192]{2,1,0:T(2,128)(2,1)}), bf16[16,2,8192]{2,1,0:T(2,128)(2,1)S(1)}, u32[]{:S(2)}, u32[]{:S(2)}) %all-to-all-start.1) | async-done | bytes 524320 | tf_op jit(solution)/shard_map/all_to_all | solution.py:86
  222.0 4.7 %multiply_reduce_fusion.1 = (f32[128]{0:T(128)S(1)}, f32[128,2048]{1,0:T(8,128)S(1)}) fusion(bf16[128,2048]{0,1:T(8,128)(2,1)S(1)} %bitcast.211, bf16[2048,2048]{1,0:T(8,128)(2,1)} %all-gather.2.cloned.1.call-done, bf16[1,128,2048]{2,1,0:T(8,128)(2,1)S(1)} %copy-done.14), kind=kOutput, calls=%fused_computation.65 | convolution fusion | flops 1075314560 | bytes 10486272 | tf_op jit(solution)/shard_map/dot_general | solution.py:87
  227.0 3.3 %gather_fusion = bf16[512,2048]{1,0:T(8,128)(2,1)} fusion(bf16[128,2048]{1,0:T(8,128)(2,1)S(1)} %multiply_convert_fusion.1, s32[1024]{0:T(1024)S(1)} %pad_clamp_fusion.1), kind=kCustom, calls=%fused_computation | custom fusion | bytes 4196352 | tf_op jit(solution)/shard_map/gather | solution.py:108
  232.1 31.1 %all_to_all.40 = bf16[16,32,2048]{2,1,0:T(8,128)(2,1)S(1)} all-to-all(bf16[16,32,2048]{2,1,0:T(8,128)(2,1)S(1)} %broadcast_select_fusion), channel_id=1, replica_groups=mesh['sp'=16,'dp'=8] {'sp'}, dimensions={0} | all-to-all | bytes 4194304 | tf_op jit(solution)/shard_map/all_to_all | solution.py:110
  263.2 3.7 %fusion.10 = f32[512,1024]{1,0:T(8,128)} fusion(bf16[512,2048]{1,0:T(8,128)(2,1)S(1)} %bitcast.216, bf16[1,2048,1024]{2,1,0:T(8,128)(2,1)S(1)} %copy-done.27), kind=kOutput, calls=%fused_computation.18 | convolution fusion | flops 2147483648 | bytes 8388608 | tf_op jit(solution)/shard_map/dot_general | solution.py:113
  266.9 9.9 %fusion.15 = bf16[512,2048]{1,0:T(8,128)(2,1)} fusion(bf16[1,1024,2048]{2,1,0:T(8,128)(2,1)} %param.21, f32[512,1024]{1,0:T(8,128)} %fusion.10, bf16[512,2048]{1,0:T(8,128)(2,1)S(1)} %bitcast.217, bf16[1,2048,1024]{2,1,0:T(8,128)(2,1)} %param.20), kind=kOutput, calls=%fused_computation.28 | convolution fusion | flops 4299161600 | bytes 14680064 | tf_op jit(solution)/shard_map/dot_general | solution.py:116
  276.8 4.1 %all-to-all-start.3 = ((bf16[16,32,2048]{2,1,0:T(8,128)(2,1)}), bf16[16,32,2048]{2,1,0:T(8,128)(2,1)S(1)}, u32[]{:S(2)}, u32[]{:S(2)}) async-start(bf16[16,32,2048]{2,1,0:T(8,128)(2,1)} %bitcast.215), calls=%async_computation.3 | async-start | bytes 4194304 | tf_op jit(solution)/shard_map/all_to_all | solution.py:117
  281.1 28.2 %all-to-all-done.3 = bf16[16,32,2048]{2,1,0:T(8,128)(2,1)S(1)} async-done(((bf16[16,32,2048]{2,1,0:T(8,128)(2,1)}), bf16[16,32,2048]{2,1,0:T(8,128)(2,1)S(1)}, u32[]{:S(2)}, u32[]{:S(2)}) %all-to-all-start.3) | async-done | bytes 2097184 | tf_op jit(solution)/shard_map/all_to_all | solution.py:117
  311.6 2.4 reshape.392
  313.9 3.2 multiply_reduce_fusion
  (142 shorter events, 62.5 us)
Async XLA Ops:
  6.5 215.5 %all-gather.2.cloned.1.call-start = ((), (), s32[]{:S(2)}) async-start(), calls=%async_computation.4 | async-start | bytes 8912896 | tf_op jit(solution)/shard_map/all_gather | solution.py:89
  18.9 8.5 %copy-start.24 = (s32[1,128,2]{1,2,0:T(2,128)S(1)}, s32[1,128,2]{1,2,0:T(2,128)}, u32[]{:S(2)}) copy-start(s32[1,128,2]{1,2,0:T(2,128)} %param.17) | copy-start | bytes 3076
  18.9 46.3 %all-to-all-start = ((bf16[3,128,2048]{1,0,2:T(4,128)(2,1)}), bf16[3,128,2048]{1,0,2:T(4,128)(2,1)}, u32[]{:S(2)}, u32[]{:S(2)}) async-start(bf16[3,128,2048]{1,0,2:T(4,128)(2,1)} %pad_maximum_fusion), calls=%async_computation | async-start | bytes 4194304 | tf_op jit(solution)/shard_map/all_to_all | solution.py:15
  29.4 49.0 %copy-start.21 = (s32[512]{0:T(512)}, s32[512]{0:T(512)S(1)}, u32[]{:S(2)}) copy-start(s32[512]{0:T(512)S(1)} %iota_add_fusion.1) | copy-start | bytes 6148
  67.7 47.5 %copy-start.4 = (bf16[3,128,2048]{1,2,0:T(8,128)(2,1)}, bf16[3,128,2048]{1,2,0:T(8,128)(2,1)S(1)}, u32[]{:S(2)}) copy-start(bf16[3,128,2048]{1,2,0:T(8,128)(2,1)S(1)} %copy.115) | copy-start | bytes 4718596
  100.8 3.7 %copy-start.2 = (f32[1,512,12,128]{1,2,3,0:T(8,128)}, f32[1,512,12,128]{1,2,3,0:T(8,128)S(1)}, u32[]{:S(2)}) copy-start(f32[1,512,12,128]{1,2,3,0:T(8,128)S(1)} %fusion.12) | copy-start | bytes 9437188
  111.1 3.9 %copy-start.16 = (bf16[1,4,128,128]{2,3,1,0:T(8,128)(2,1)S(1)}, bf16[1,4,128,128]{2,3,1,0:T(8,128)(2,1)}, u32[]{:S(2)}) copy-start(bf16[1,4,128,128]{2,3,1,0:T(8,128)(2,1)} %get-tuple-element.51) | copy-start | bytes 393220
  130.1 5.6 %copy-start.15 = (bf16[1,4,128,128]{2,3,1,0:T(8,128)(2,1)S(1)}, bf16[1,4,128,128]{2,3,1,0:T(8,128)(2,1)}, u32[]{:S(2)}) copy-start(bf16[1,4,128,128]{2,3,1,0:T(8,128)(2,1)} %get-tuple-element.44) | copy-start | bytes 393220
  138.9 1.6 copy-start.18
  140.5 3.0 copy-start
  165.1 14.0 %copy-start.8 = (f32[1,512,4,128]{1,3,2,0:T(8,128)S(1)}, f32[1,512,4,128]{1,3,2,0:T(8,128)}, u32[]{:S(2)}) copy-start(f32[1,512,4,128]{1,3,2,0:T(8,128)} %copy.120) | copy-start | bytes 3145732
  179.1 2.9 copy-start.12
  179.1 3.5 %copy-start.7 = (f32[1,512,8,128]{3,2,1,0:T(8,128)S(1)}, f32[1,512,8,128]{3,2,1,0:T(8,128)}, u32[]{:S(2)}) copy-start(f32[1,512,8,128]{3,2,1,0:T(8,128)} %copy.125) | copy-start | bytes 6291460
  179.1 3.5 %copy-start.11 = (bf16[1,8,128,128]{3,2,1,0:T(8,128)(2,1)S(1)}, bf16[1,8,128,128]{3,2,1,0:T(8,128)(2,1)}, u32[]{:S(2)}) copy-start(bf16[1,8,128,128]{3,2,1,0:T(8,128)(2,1)} %copy.121) | copy-start | bytes 786436
  179.1 3.5 %copy-start.17 = (s32[512]{0:T(512)S(1)}, s32[512]{0:T(512)}, u32[]{:S(2)}) copy-start(s32[512]{0:T(512)} %iota_add_fusion.2) | copy-start | bytes 6148
  180.6 3.3 %copy-start.9 = (f32[512,1536]{1,0:T(8,128)S(1)}, f32[512,1536]{1,0:T(8,128)}, u32[]{:S(2)}) copy-start(f32[512,1536]{1,0:T(8,128)} %get-tuple-element.71) | copy-start | bytes 9437188
  182.6 1.9 copy-start.5
  182.6 2.8 copy-start.6
  182.6 2.8 copy-start.22
  185.4 1.2 copy-start.13
  185.4 2.4 copy-start.3
  185.4 2.4 copy-start.10
  186.7 2.7 copy-start.1
  186.7 2.7 copy-start.19
  192.6 17.4 %copy-start.23 = (s32[256,1]{0,1:T(1,128)S(1)}, s32[256,1]{0,1:T(1,128)}, u32[]{:S(2)}) copy-start(s32[256,1]{0,1:T(1,128)} %mul.83) | copy-start | bytes 3076
  192.6 17.4 %copy-start.25 = (s32[256]{0:T(256)S(1)}, s32[256]{0:T(256)}, u32[]{:S(2)}) copy-start(s32[256]{0:T(256)} %fusion.54) | copy-start | bytes 3076
  205.5 16.5 %copy-start.14 = (bf16[1,128,2048]{2,1,0:T(8,128)(2,1)S(1)}, bf16[1,128,2048]{2,1,0:T(8,128)(2,1)}, u32[]{:S(2)}) copy-start(bf16[1,128,2048]{2,1,0:T(8,128)(2,1)} %param.15) | copy-start | bytes 1572868
  206.4 14.7 %all-to-all-start.1 = ((bf16[16,2,8192]{2,1,0:T(2,128)(2,1)}), bf16[16,2,8192]{2,1,0:T(2,128)(2,1)S(1)}, u32[]{:S(2)}, u32[]{:S(2)}) async-start(bf16[16,2,8192]{2,1,0:T(2,128)(2,1)} %reshape.431), calls=%async_computation.1 | async-start | bytes 1048576 | tf_op jit(solution)/shard_map/all_to_all | solution.py:86
  222.0 4.8 %copy-start.20 = (f32[2048]{0:T(1024)S(1)}, f32[2048]{0:T(1024)}, u32[]{:S(2)}) copy-start(f32[2048]{0:T(1024)} %param.16) | copy-start | bytes 24580
  232.1 31.1 %copy-start.27 = (bf16[1,2048,1024]{2,1,0:T(8,128)(2,1)S(1)}, bf16[1,2048,1024]{2,1,0:T(8,128)(2,1)}, u32[]{:S(2)}) copy-start(bf16[1,2048,1024]{2,1,0:T(8,128)(2,1)} %param.19) | copy-start | bytes 12582916
  276.8 4.1 %copy-start.26 = (f32[1,128,2]{1,2,0:T(2,128)S(1)}, f32[1,128,2]{1,2,0:T(2,128)}, u32[]{:S(2)}) copy-start(f32[1,128,2]{1,2,0:T(2,128)} %param.18) | copy-start | bytes 3076
  276.8 32.4 %all-to-all-start.3 = ((bf16[16,32,2048]{2,1,0:T(8,128)(2,1)}), bf16[16,32,2048]{2,1,0:T(8,128)(2,1)S(1)}, u32[]{:S(2)}, u32[]{:S(2)}) async-start(bf16[16,32,2048]{2,1,0:T(8,128)(2,1)} %bitcast.215), calls=%async_computation.3 | async-start | bytes 4194304 | tf_op jit(solution)/shard_map/all_to_all | solution.py:117
Sparse Core Ops, SparseCore 0:
  9.5 93.7 all-gather.1
where the time goes:
time: 329 us; the launch traced here: 325 us
  local copies, waits for them, and re-layouts  87.9 us (27%)
  waiting for transfers between devices  70.7 us (21%)
  other arithmetic  69.5 us (21%)
  matrix products  35.4 us (11%)
  blocking collectives  31.1 us (9%)
  starting transfers between devices  16.2 us (5%)
  between operations  14.3 us (4%)
    another operation x23, local copies, waits for them, and re-layouts  41.4 us
    another operation x10, other arithmetic  38.8 us
    all_to_all x1, waiting for transfers between devices, sent_together(): lax.all_to_all(both, axis, split_axis=split_dim, concat_axis=concat_dim,...  34 us
    all_to_all x1, blocking collectives, body(): lax.all_to_all(outgoing, 'sp', split_axis=0, concat_axis=0, tiled=True)  31.1 us
    all_to_all x1, waiting for transfers between devices, body(): lax.all_to_all(result.reshape(senders, slots, features), 'sp', split_axis...  28.2 us
    unnamed x66, local copies, waits for them, and re-layouts  16.9 us
    unnamed x3, other arithmetic  16.7 us
    dot_general x4, matrix products, one_block(): jnp.einsum('qhd,khd->hqk', query_block, near_keys, preferred_element_type...  10 us
  transfers between devices with their start and end apart: 4, of which 3 were waited for; matrix products, arithmetic and copies ran while one was open for 48% of the time, Pallas kernels for 0%

commit v1 on v0

v1 whole, which is shorter than its diff:
```python
import functools
import math

import jax
import jax.numpy as jnp
from jax import lax
from jax.experimental import pallas as pl
from jax.experimental.pallas import tpu as pltpu
from jax.sharding import PartitionSpec as P

MESH = pl.DeviceIdType.MESH
EPS = 1e-06
SIDE = 4
N_SP = 16
ROWS = 128
HEAD = 128
LENGTH = 2048
WIDTH = 2048
FFE = 1024
CAP = 32
TILE = 256
LOG2E = 1.0 / math.log(2.0)

SHIFTS = (
    (1, 2), (3, 2), (2, 1), (2, 3),
    (2, 2), (2, 0), (0, 2), (0, 0),
    (1, 1), (3, 3), (1, 3), (3, 1),
    (1, 0), (3, 0), (0, 1), (0, 3),
)
OWN = SHIFTS.index((0, 0))
GROUPS = 4
PER_GROUP = 4
GROUP_ROWS = PER_GROUP * CAP


def dot(a, b):
    return jnp.dot(a, b, preferred_element_type=jnp.float32)


def body_kernel(
    q_hbm, k_hbm, v_hbm, proj_hbm, res_hbm, gain_ref, route_ref, rw_ref,
    wg_hbm, wu_hbm, wd_hbm,
    out_ref,
    qh, kh, vh, w_att, carry, tri, o_buf, oa, ob, proj_a, proj_b,
    part_a, part_b, sum_a, sum_b, res, acc, normed, pick, mix_hi, mix_lo,
    xs, xr, ys, yr, hid, wg, wu, wd,
    local_sem, head_send, head_recv, proj_send, proj_recv, o_send, o_recv,
    r_send, r_recv, d_send, d_recv, y_send, y_recv,
):
    me = lax.axis_index("sp")
    z = me // SIDE
    y = me % SIDE

    def at(a, b):
        return ((z + a) % SIDE) * SIDE + (y + b) % SIDE

    others = [s for s in SHIFTS if s != (0, 0)]
    line = (2, 1, 3)

    barrier = pltpu.get_barrier_semaphore()
    for a, b in others:
        pl.semaphore_signal(barrier, inc=1, device_id={"sp": at(a, b)}, device_id_type=MESH)

    def local(src, dst, sem):
        copy = pltpu.make_async_copy(src, dst, sem)
        copy.start()
        return copy

    def remote(src, dst, send, recv, peer):
        pltpu.make_async_remote_copy(
            src_ref=src, dst_ref=dst, send_sem=send, recv_sem=recv,
            device_id={"sp": peer}, device_id_type=MESH,
        ).start()

    def wait_for(ref, sem):
        pltpu.make_async_copy(ref, ref, sem).wait()

    my_rows = pl.ds(pl.multiple_of(me * ROWS, ROWS), ROWS)

    def cols(peer):
        return pl.ds(pl.multiple_of(peer * HEAD, HEAD), HEAD)

    heads = ((k_hbm, kh), (q_hbm, qh), (v_hbm, vh))
    for t, (src, dst) in enumerate(heads):
        local(src.at[0, :, cols(me)], dst.at[my_rows], head_recv.at[t])
    local(proj_hbm.at[:, pl.ds(0, 1024)], proj_a.at[y], proj_recv.at[0])
    local(proj_hbm.at[:, pl.ds(1024, 1024)], proj_b.at[z], proj_recv.at[1])

    pl.semaphore_wait(barrier, N_SP - 1)

    def send_heads(t, a, b):
        src, dst = heads[t]
        peer = at(a, b)
        remote(src.at[0, :, cols(peer)], dst.at[my_rows], head_send.at[t], head_recv.at[t], peer)

    for a, b in others:
        send_heads(0, a, b)
        send_heads(1, a, b)
    for a, b in others:
        send_heads(2, a, b)
    for s in line:
        remote(proj_hbm.at[:, pl.ds(0, 1024)], proj_a.at[y], proj_send.at[0], proj_recv.at[0], at(0, s))
        remote(proj_hbm.at[:, pl.ds(1024, 1024)], proj_b.at[z], proj_send.at[1], proj_recv.at[1], at(s, 0))
    loads = [
        local(res_hbm.at[0], res, local_sem.at[0]),
        local(wg_hbm.at[0], wg, local_sem.at[1]),
        local(wu_hbm.at[0], wu, local_sem.at[2]),
        local(wd_hbm.at[0], wd, local_sem.at[3]),
    ]

    j = lax.broadcasted_iota(jnp.int32, (TILE, TILE + HEAD), 0)
    s = lax.broadcasted_iota(jnp.int32, (TILE, TILE + HEAD), 1)
    tri[...] = jnp.where((j > s) | (s >= TILE), 1.0, 0.0).astype(jnp.bfloat16)

    @pl.loop(0, LENGTH // 64)
    def _(i):
        w_att[pl.ds(pl.multiple_of(i * 64, 64), 64), :] = jnp.zeros((64, LENGTH), jnp.bfloat16)

    slots = N_SP * CAP
    lane = lax.broadcasted_iota(jnp.int32, (ROWS, slots), 1)
    place = lane // CAP
    expert = jnp.zeros((ROWS, slots), jnp.int32)
    for i, (a, b) in enumerate(SHIFTS):
        expert = jnp.where(place == i, at(a, b), expert)
    first = route_ref[0, :, 0:1] == expert
    second = route_ref[0, :, 1:2] == expert
    named = jnp.where(first | second, 1.0, 0.0)
    r0 = lax.broadcasted_iota(jnp.int32, (ROWS, ROWS), 0)
    r1 = lax.broadcasted_iota(jnp.int32, (ROWS, ROWS), 1)
    before = jnp.where(r1 < r0, 1.0, 0.0).astype(jnp.bfloat16)
    slot = dot(before, named.astype(jnp.bfloat16))
    held = jnp.where(slot == (lane - place * CAP).astype(jnp.float32), named, 0.0)
    pick[...] = held.T.astype(jnp.bfloat16)
    mix = held * jnp.where(first, rw_ref[0, :, 0:1], rw_ref[0, :, 1:2])
    high = mix.astype(jnp.bfloat16)
    mix_hi[...] = high
    mix_lo[...] = (mix - high.astype(jnp.float32)).astype(jnp.bfloat16)

    wait_for(kh, head_recv.at[0])
    wait_for(qh, head_recv.at[1])
    scale = HEAD ** (-0.5) * LOG2E

    def weights(q0, k0, diagonal):
        q_rows = pl.ds(q0, TILE)
        k_rows = pl.ds(k0, TILE)
        u = lax.dot_general(
            qh[q_rows, :], kh[k_rows, :], (((1,), (1,)), ((), ())),
            preferred_element_type=jnp.float32,
        ) * scale
        low = jnp.log(1.0 + jnp.exp2(-jnp.abs(u))) * LOG2E
        soft = jnp.maximum(u, 0.0) + low
        if diagonal:
            causal = lax.broadcasted_iota(jnp.int32, (TILE, TILE), 1) < lax.broadcasted_iota(
                jnp.int32, (TILE, TILE), 0
            )
            soft = jnp.where(causal, soft, 0.0)
        sums = dot(soft.astype(jnp.bfloat16), tri[...])
        power = jnp.minimum(u, 0.0) - low - sums[:, :TILE]
        total = sums[:, TILE:]
        if not diagonal:
            later = carry[q_rows, :]
            power = power - jnp.concatenate([later, later], axis=1)
            total = total + later
        weight = jnp.exp2(power)
        if diagonal:
            weight = jnp.where(causal, weight, 0.0)
        w_att[q_rows, k_rows] = weight.astype(jnp.bfloat16)
        carry[q_rows, :] = total

    @pl.loop(0, 4)
    def _(i):
        for half in range(2):
            base = pl.multiple_of(i * 512 + half * TILE, TILE)
            weights(base, base, True)

    @pl.loop(0, 2)
    def _(i):
        for half in range(2):
            base = pl.multiple_of(i * 1024 + half * 512, TILE)
            weights(base + TILE, base, False)

    for big in range(1, 4):
        @pl.loop(0, 2 * big)
        def _(i):
            k0 = pl.multiple_of((2 * big - 1 - i) * TILE, TILE)
            for half in range(2):
                weights(big * 512 + half * TILE, k0, False)

    wait_for(vh, head_recv.at[2])
    for i in range(SIDE):
        quarter = (z + 1 + i) % SIDE
        rows = pl.ds(pl.multiple_of(quarter * 512, 512), 512)
        o_buf[quarter] = dot(w_att[rows, :], vh[...]).astype(jnp.bfloat16).reshape(SIDE, ROWS, HEAD)
        if i < SIDE - 1:
            remote(o_buf.at[quarter], ob.at[:, :, cols(z)], o_send.at[1], o_recv.at[1], quarter * SIDE + y)
    for s in line:
        peer_y = (y + s) % SIDE
        remote(o_buf.at[:, peer_y], oa.at[:, :, cols(y)], o_send.at[0], o_recv.at[0], z * SIDE + peer_y)
    ob[:, :, cols(z)] = o_buf[z]
    for i in range(SIDE):
        oa[i, :, cols(y)] = o_buf[i, y]

    def project(index, o_in, weight, part):
        wait_for(weight, proj_recv.at[index])
        wait_for(o_in.at[:, :, pl.ds(0, 3 * HEAD)], o_recv.at[index])
        left = o_in[...].reshape(512, 512)

        @pl.loop(0, 1024 // TILE)
        def _(n):
            c = pl.ds(pl.multiple_of(n * TILE, TILE), TILE)
            right = weight[:, :, c].reshape(512, TILE)
            part[:, :, c] = dot(left, right).astype(jnp.bfloat16).reshape(SIDE, ROWS, TILE)

    project(1, ob, proj_b, part_b)
    for s in line:
        peer_y = (y + s) % SIDE
        remote(part_b.at[peer_y], sum_b.at[y], r_send.at[1], r_recv.at[1], z * SIDE + peer_y)
    project(0, oa, proj_a, part_a)
    for s in line:
        peer_z = (z + s) % SIDE
        remote(part_a.at[peer_z], sum_a.at[z], r_send.at[0], r_recv.at[0], peer_z * SIDE + y)
    sum_b[y] = part_b[y]
    sum_a[z] = part_a[z]
    loads[0].wait()
    wait_for(sum_b.at[pl.ds(0, 3)], r_recv.at[1])
    wait_for(sum_a.at[pl.ds(0, 3)], r_recv.at[0])

    @pl.loop(0, ROWS // 16)
    def _(i):
        r = pl.ds(pl.multiple_of(i * 16, 16), 16)
        halves = []
        for h, sums in enumerate((sum_a, sum_b)):
            total = res[r, h * 1024:(h + 1) * 1024].astype(jnp.float32)
            for k in range(SIDE):
                total = total + sums[k, r, :].astype(jnp.float32)
            halves.append(total.astype(jnp.bfloat16).astype(jnp.float32))
        stream = jnp.concatenate(halves, axis=1)
        acc[r, :] = stream
        mean = jnp.mean(stream * stream, axis=-1, keepdims=True)
        normed[r, :] = (stream * lax.rsqrt(mean + EPS) * gain_ref[...]).astype(jnp.bfloat16)

    for g in range(GROUPS):
        @pl.loop(0, WIDTH // 512)
        def _(n):
            c = pl.ds(pl.multiple_of(n * 512, 512), 512)
            rows = dot(pick[g * GROUP_ROWS:(g + 1) * GROUP_ROWS, :], normed[:, c])
            rows = rows.astype(jnp.bfloat16).reshape(PER_GROUP, CAP, 512)
            xs[g * PER_GROUP:(g + 1) * PER_GROUP, :, c] = rows

        for i in range(g * PER_GROUP, (g + 1) * PER_GROUP):
            if i == OWN:
                xr[i] = xs[i]
            else:
                remote(xs.at[i], xr.at[i], d_send, d_recv.at[g], at(*SHIFTS[i]))

    loads[1].wait()
    loads[2].wait()
    loads[3].wait()

    def remote_count(g):
        return PER_GROUP - (1 if OWN // PER_GROUP == g else 0)

    for g in range(GROUPS):
        mine = slice(g * PER_GROUP, (g + 1) * PER_GROUP)
        wait_for(xr.at[pl.ds(g * PER_GROUP, remote_count(g))], d_recv.at[g])

        @pl.loop(0, FFE // TILE)
        def _(n):
            c = pl.ds(pl.multiple_of(n * TILE, TILE), TILE)
            x = xr[mine].reshape(GROUP_ROWS, WIDTH)
            gate = dot(x, wg[:, c])
            upper = dot(x, wu[:, c])
            hid[:, c] = (gate / (1.0 + jnp.exp(-gate)) * upper).astype(jnp.bfloat16)

        @pl.loop(0, WIDTH // 512)
        def _(n):
            c = pl.ds(pl.multiple_of(n * 512, 512), 512)
            result = dot(hid[...], wd[:, c]).astype(jnp.bfloat16)
            ys[mine, :, c] = result.reshape(PER_GROUP, CAP, 512)

        for i in range(g * PER_GROUP, (g + 1) * PER_GROUP):
            if i == OWN:
                yr[i] = ys[i]
            else:
                a, b = SHIFTS[i]
                remote(ys.at[i], yr.at[i], y_send, y_recv.at[g], at(-a, -b))

    for g in range(GROUPS):
        wait_for(yr.at[pl.ds(g * PER_GROUP, remote_count(g))], y_recv.at[g])

        @pl.loop(0, WIDTH // 512)
        def _(n):
            c = pl.ds(pl.multiple_of(n * 512, 512), 512)
            lanes = slice(g * GROUP_ROWS, (g + 1) * GROUP_ROWS)
            got = yr[g * PER_GROUP:(g + 1) * PER_GROUP, :, c].reshape(GROUP_ROWS, 512)
            total = acc[:, c] + dot(mix_hi[:, lanes], got) + dot(mix_lo[:, lanes], got)
            if g < GROUPS - 1:
                acc[:, c] = total
            else:
                out_ref[0, :, c] = total.astype(jnp.bfloat16)

    fifteen = pl.ds(0, N_SP - 1)
    for t, (src, dst) in enumerate(heads):
        wait_for(dst.at[pl.ds(0, ROWS * (N_SP - 1))], head_send.at[t])
    for i in range(2):
        wait_for(proj_a.at[pl.ds(0, 3)], proj_send.at[i])
        wait_for(o_buf.at[pl.ds(0, 3)], o_send.at[i])
        wait_for(part_a.at[pl.ds(0, 3)], r_send.at[i])
    wait_for(xs.at[fifteen], d_send)
    wait_for(ys.at[fifteen], y_send)


def body(
    queries, keys, values, proj_weight, residual, norm_gain, route, route_weight,
    w_gate, w_up, w_down,
):
    bf16, f32 = jnp.bfloat16, jnp.float32
    vmem = pltpu.VMEM
    dma = pltpu.SemaphoreType.DMA
    anywhere = pl.BlockSpec(memory_space=pl.ANY)
    inside = pl.BlockSpec(memory_space=pltpu.VMEM)
    scratch = [
        vmem((LENGTH, HEAD), bf16), vmem((LENGTH, HEAD), bf16), vmem((LENGTH, HEAD), bf16),
        vmem((LENGTH, LENGTH), bf16), vmem((LENGTH, HEAD), f32), vmem((TILE, TILE + HEAD), bf16),
        vmem((SIDE, SIDE, ROWS, HEAD), bf16),
        vmem((SIDE, ROWS, 512), bf16), vmem((SIDE, ROWS, 512), bf16),
        vmem((SIDE, ROWS, 1024), bf16), vmem((SIDE, ROWS, 1024), bf16),
        vmem((SIDE, ROWS, 1024), bf16), vmem((SIDE, ROWS, 1024), bf16),
        vmem((SIDE, ROWS, 1024), bf16), vmem((SIDE, ROWS, 1024), bf16),
        vmem((ROWS, WIDTH), bf16), vmem((ROWS, WIDTH), f32), vmem((ROWS, WIDTH), bf16),
        vmem((N_SP * CAP, ROWS), bf16), vmem((ROWS, N_SP * CAP), bf16), vmem((ROWS, N_SP * CAP), bf16),
        vmem((N_SP, CAP, WIDTH), bf16), vmem((N_SP, CAP, WIDTH), bf16),
        vmem((N_SP, CAP, WIDTH), bf16), vmem((N_SP, CAP, WIDTH), bf16),
        vmem((GROUP_ROWS, FFE), bf16),
        vmem((WIDTH, FFE), bf16), vmem((WIDTH, FFE), bf16), vmem((FFE, WIDTH), bf16),
        dma((4,)), dma((3,)), dma((3,)), dma((2,)), dma((2,)), dma((2,)), dma((2,)),
        dma((2,)), dma((2,)), dma, dma((GROUPS,)), dma, dma((GROUPS,)),
    ]
    return pl.pallas_call(
        body_kernel,
        out_shape=jax.ShapeDtypeStruct((1, ROWS, WIDTH), bf16),
        in_specs=[anywhere] * 5 + [inside] * 3 + [anywhere] * 3,
        out_specs=inside,
        scratch_shapes=scratch,
        compiler_params=pltpu.CompilerParams(
            collective_id=0, has_side_effects=True, vmem_limit_bytes=62 * 1024 * 1024
        ),
        name="layer",
    )(
        queries, keys, values, proj_weight, residual, norm_gain.reshape(1, WIDTH), route,
        route_weight, w_gate, w_up, w_down,
    )


def solution(mesh):
    return jax.shard_map(
        body,
        mesh=mesh,
        in_specs=(
            P("dp", "sp", None),
            P("dp", "sp", None),
            P("dp", "sp", None),
            P("sp", None),
            P("dp", "sp", None),
            P(),
            P("dp", "sp", None),
            P("dp", "sp", None),
            P("sp", None, None),
            P("sp", None, None),
            P("sp", None, None),
        ),
        out_specs=P("dp", "sp", None),
        check_vma=False,
    )
```

time: 329 us -> 121 us (0.37); the launches traced: 325 us -> 121 us
  Pallas kernels: 0 us -> 116 us
  local copies, waits for them, and re-layouts: 87.9 us -> 4.7 us
  waiting for transfers between devices: 70.7 us -> 0 us
  other arithmetic: 69.5 us -> 0 us
  matrix products: 35.4 us -> 0 us
  blocking collectives: 31.1 us -> 0 us
  starting transfers between devices: 16.2 us -> 0 us
  between operations: 14.3 us -> 0.01 us
    pallas_call x0 -> x1, Pallas kernels: none -> 116 us  [body(): pl.pallas_call(body_kernel, out_shape=jax.ShapeDtypeStruct((1, ROWS, WIDT...]
    all_to_all x3 -> x0, waiting for transfers between devices: 70 us -> none  [the longest x1 34 us: sent_together(): lax.all_to_all(both, axis, split_axis=split_dim, concat_axis=concat_dim,...]
    another operation x23 -> x0, local copies, waits for them, and re-layouts: 41.4 us -> none
    another operation x10 -> x0, other arithmetic: 38.8 us -> none
    dot_general x11 -> x0, matrix products: 35.4 us -> none  [the longest x4 10 us: one_block(): jnp.einsum('qhd,khd->hqk', query_block, near_keys, preferred_element_type...]
    all_to_all x1 -> x0, blocking collectives: 31.1 us -> none  [body(): lax.all_to_all(outgoing, 'sp', split_axis=0, concat_axis=0, tiled=True)]
    unnamed x3 -> x0, other arithmetic: 16.7 us -> none
    all_to_all x3 -> x0, starting transfers between devices: 16.2 us -> none  [the longest x1 8.53 us: sent_together(): lax.all_to_all(both, axis, split_axis=split_dim, concat_axis=concat_dim,...]
  transfers between devices with their start and end apart: 4 -> 0, of which waited for: 3 -> 0; matrix products, arithmetic and copies ran while one was open for 48% -> 0% of each run, Pallas kernels for 0% -> 0%
where the time goes in v1:
time: 121 us
  Pallas kernels  116 us (96%)
  local copies, waits for them, and re-layouts  4.7 us (4%)
    pallas_call x1, Pallas kernels, body(): pl.pallas_call(body_kernel, out_shape=jax.ShapeDtypeStruct((1, ROWS, WIDT...  116 us
    unnamed x3, local copies, waits for them, and re-layouts  4.7 us

profile of v1, /device:TPU:0, one launch (start us, length us, event | category | flops | bytes accessed | tf_op | source)
XLA Modules:
  0.0 121.0 jit_solution(18287375286580751263)
XLA Ops:
  0.0 1.4 %copy.12.route_ref = s32[1,128,2]{2,1,0:T(8,128)} copy(s32[1,128,2]{1,2,0:T(2,128)} %param.17) | data formatting | bytes 2048 | tf_op args[6]
  1.4 1.4 %copy.13.rw_ref = f32[1,128,2]{2,1,0:T(8,128)} copy(f32[1,128,2]{1,2,0:T(2,128)} %param.18) | data formatting | bytes 2048 | tf_op args[7]
  2.8 116.3 %layer.1 = bf16[1,128,2048]{2,1,0:T(8,128)(2,1)} custom-call(bf16[1,128,2048]{2,1,0:T(8,128)(2,1)} %q_hbm.1, bf16[1,128,2048]{2,1,0:T(8,128)(2,1)} %k_hbm.1, bf16[1,128,2048]{2,1,0:T(8,128)(2,1)} %v_hbm.1, bf16[128,2048]{1,0:T(8,128)(2,1)} %proj_hbm.1, bf16[1,128,2048]{2,1,0:T(8,128)(2,1)} %res_hbm.1, f32[1,2048]{1,0:T(1,128)} %bitcast.1, ...), custom_call_target="tpu_custom_call" | custom-call | tf_op jit(solution)/shard_map/layer/pallas_call | solution.py:339
  119.1 1.9 %copy.15 = bf16[1,128,2048]{2,1,0:T(8,128)(2,1)} copy(bf16[1,128,2048]{2,1,0:T(8,128)(2,1)} %layer.1) | data formatting | bytes 1048576

commit v2 on v1

v2 whole, which is shorter than its diff:
```python
import functools
import math

import jax
import jax.numpy as jnp
from jax import lax
from jax.experimental import pallas as pl
from jax.experimental.pallas import tpu as pltpu
from jax.sharding import PartitionSpec as P

MESH = pl.DeviceIdType.MESH
EPS = 1e-06
SIDE = 4
N_SP = 16
ROWS = 128
HEAD = 128
LENGTH = 2048
WIDTH = 2048
FFE = 1024
HALF = 1024
CHUNK = 512
CHUNKS = 4
CAP = 32
TILE = 256
LOG2E = 1.0 / math.log(2.0)

SHIFTS = (
    (1, 2), (3, 2), (2, 1), (2, 3),
    (2, 2), (2, 0), (0, 2), (0, 0),
    (1, 1), (3, 3), (1, 3), (3, 1),
    (1, 0), (3, 0), (0, 1), (0, 3),
)
OWN = SHIFTS.index((0, 0))
GROUPS = 4
PER_GROUP = 4
GROUP_ROWS = PER_GROUP * CAP


def dot(a, b):
    return jnp.dot(a, b, preferred_element_type=jnp.float32)


def body_kernel(
    q_hbm, k_hbm, v_hbm, proj_hbm, res_hbm, gain_ref, route_ref, rw_ref,
    wg_hbm, wu_hbm, wd_hbm,
    out_ref,
    qh, kh, vh, w_att, carry, tri, o_buf, oa, ob, proj_a, proj_b,
    part_a, part_b, sum_a, sum_b, res, acc, pick, mix_hi, mix_lo,
    xs, xr, ys, yr, scaled, squares, gate_acc, up_acc, hid, wg, wu, wd,
    local_sem, head_send, head_recv, proj_send, proj_recv, relay_send, relay_recv,
    o_send, oa_recv, ob_recv, r_send, ra_recv, rb_recv, d_send, d_recv, y_send, y_recv,
):
    me = lax.axis_index("sp")
    dp = lax.axis_index("dp")
    z = me // SIDE
    y = me % SIDE
    core = dp % 2
    partner = dp + 1 - 2 * core

    def at(a, b):
        return ((z + a) % SIDE) * SIDE + (y + b) % SIDE

    others = [s for s in SHIFTS if s != (0, 0)]
    line = (2, 1, 3)

    barrier = pltpu.get_barrier_semaphore()
    for a, b in others:
        pl.semaphore_signal(barrier, inc=1, device_id={"sp": at(a, b)}, device_id_type=MESH)
    pl.semaphore_signal(barrier, inc=1, device_id={"dp": partner}, device_id_type=MESH)

    def local(src, dst, sem):
        copy = pltpu.make_async_copy(src, dst, sem)
        copy.start()
        return copy

    def remote(src, dst, send, recv, peer, axis="sp"):
        pltpu.make_async_remote_copy(
            src_ref=src, dst_ref=dst, send_sem=send, recv_sem=recv,
            device_id={axis: peer}, device_id_type=MESH,
        ).start()

    def wait_for(ref, sem):
        pltpu.make_async_copy(ref, ref, sem).wait()

    my_rows = pl.ds(pl.multiple_of(me * ROWS, ROWS), ROWS)
    core_rows = pl.ds(pl.multiple_of(core * (ROWS // 2), ROWS // 2), ROWS // 2)

    def cols(peer):
        return pl.ds(pl.multiple_of(peer * HEAD, HEAD), HEAD)

    heads = ((k_hbm, kh), (q_hbm, qh), (v_hbm, vh))
    for t, (src, dst) in enumerate(heads):
        local(src.at[0, :, cols(me)], dst.at[my_rows], head_recv.at[t])
    loads = [
        local(proj_hbm.at[:, pl.ds(0, HALF)], proj_a.at[y], local_sem.at[4]),
        local(proj_hbm.at[:, pl.ds(HALF, HALF)], proj_b.at[z], local_sem.at[5]),
    ]

    pl.semaphore_wait(barrier, N_SP)

    def send_heads(t, a, b):
        src, dst = heads[t]
        peer = at(a, b)
        remote(src.at[0, :, cols(peer)], dst.at[my_rows], head_send.at[t], head_recv.at[t], peer)

    for a, b in others:
        send_heads(0, a, b)
        send_heads(1, a, b)
    for a, b in others:
        send_heads(2, a, b)
    for s in line:
        remote(proj_hbm.at[core_rows, pl.ds(0, HALF)], proj_a.at[y, core_rows],
               proj_send.at[0], proj_recv.at[0], at(0, s))
    for s in line:
        remote(proj_hbm.at[core_rows, pl.ds(HALF, HALF)], proj_b.at[z, core_rows],
               proj_send.at[1], proj_recv.at[1], at(s, 0))
    loads += [
        local(res_hbm.at[0], res, local_sem.at[0]),
        local(wg_hbm.at[0], wg, local_sem.at[1]),
        local(wu_hbm.at[0], wu, local_sem.at[2]),
        local(wd_hbm.at[0], wd, local_sem.at[3]),
    ]

    j = lax.broadcasted_iota(jnp.int32, (TILE, TILE + HEAD), 0)
    s = lax.broadcasted_iota(jnp.int32, (TILE, TILE + HEAD), 1)
    tri[...] = jnp.where((j > s) | (s >= TILE), 1.0, 0.0).astype(jnp.bfloat16)

    @pl.loop(0, LENGTH // 64)
    def _(i):
        w_att[pl.ds(pl.multiple_of(i * 64, 64), 64), :] = jnp.zeros((64, LENGTH), jnp.bfloat16)

    slots = N_SP * CAP
    lane = lax.broadcasted_iota(jnp.int32, (ROWS, slots), 1)
    place = lane // CAP
    expert = jnp.zeros((ROWS, slots), jnp.int32)
    for i, (a, b) in enumerate(SHIFTS):
        expert = jnp.where(place == i, at(a, b), expert)
    zeros = jnp.zeros((6, ROWS), jnp.float32)
    route = jnp.concatenate([route_ref[0].astype(jnp.float32), zeros], axis=0).T
    share = jnp.concatenate([rw_ref[0], zeros], axis=0).T
    expert = expert.astype(jnp.float32)
    first = route[:, 0:1] == expert
    second = route[:, 1:2] == expert
    named = jnp.where(first | second, 1.0, 0.0)
    r0 = lax.broadcasted_iota(jnp.int32, (ROWS, ROWS), 0)
    r1 = lax.broadcasted_iota(jnp.int32, (ROWS, ROWS), 1)
    before = jnp.where(r1 < r0, 1.0, 0.0).astype(jnp.bfloat16)
    slot = dot(before, named.astype(jnp.bfloat16))
    held = jnp.where(slot == (lane - place * CAP).astype(jnp.float32), named, 0.0)
    pick[...] = held.T.astype(jnp.bfloat16)
    mix = held * jnp.where(first, share[:, 0:1], share[:, 1:2])
    high = mix.astype(jnp.bfloat16)
    mix_hi[...] = high
    mix_lo[...] = (mix - high.astype(jnp.float32)).astype(jnp.bfloat16)

    wait_for(kh, head_recv.at[0])
    wait_for(qh, head_recv.at[1])
    scale = HEAD ** (-0.5) * LOG2E

    def weights(q0, k0, diagonal):
        q_rows = pl.ds(q0, TILE)
        k_rows = pl.ds(k0, TILE)
        u = lax.dot_general(
            qh[q_rows, :], kh[k_rows, :], (((1,), (1,)), ((), ())),
            preferred_element_type=jnp.float32,
        ) * scale
        low = jnp.log(1.0 + jnp.exp2(-jnp.abs(u))) * LOG2E
        soft = jnp.maximum(u, 0.0) + low
        if diagonal:
            causal = lax.broadcasted_iota(jnp.int32, (TILE, TILE), 1) < lax.broadcasted_iota(
                jnp.int32, (TILE, TILE), 0
            )
            soft = jnp.where(causal, soft, 0.0)
        sums = dot(soft.astype(jnp.bfloat16), tri[...])
        power = jnp.minimum(u, 0.0) - low - sums[:, :TILE]
        total = sums[:, TILE:]
        if not diagonal:
            later = carry[q_rows, :]
            power = power - jnp.concatenate([later, later], axis=1)
            total = total + later
        weight = jnp.exp2(power)
        if diagonal:
            weight = jnp.where(causal, weight, 0.0)
        w_att[q_rows, k_rows] = weight.astype(jnp.bfloat16)
        carry[q_rows, :] = total

    @pl.loop(0, 4)
    def _(i):
        for half in range(2):
            base = pl.multiple_of(i * 512 + half * TILE, TILE)
            weights(base, base, True)

    @pl.loop(0, 2)
    def _(i):
        for half in range(2):
            base = pl.multiple_of(i * 1024 + half * 512, TILE)
            weights(base + TILE, base, False)

    for big in range(1, 4):
        @pl.loop(0, 2 * big)
        def _(i):
            k0 = pl.multiple_of((2 * big - 1 - i) * TILE, TILE)
            for half in range(2):
                weights(big * 512 + half * TILE, k0, False)

    wait_for(vh, head_recv.at[2])
    for i in range(SIDE):
        quarter = (z + 1 + i) % SIDE
        rows = pl.ds(pl.multiple_of(quarter * 512, 512), 512)
        o_buf[quarter] = dot(w_att[rows, :], vh[...]).astype(jnp.bfloat16).reshape(SIDE, ROWS, HEAD)
        if i < SIDE - 1:
            remote(o_buf.at[quarter], ob.at[:, :, cols(z)], o_send.at[1], ob_recv, quarter * SIDE + y)
        else:
            ob[:, :, cols(z)] = o_buf[z]
        for s in line:
            peer_y = (y + s) % SIDE
            remote(o_buf.at[quarter, peer_y], oa.at[quarter, :, cols(y)], o_send.at[0],
                   oa_recv.at[quarter], z * SIDE + peer_y)
        oa[quarter, :, cols(y)] = o_buf[quarter, y]

    three = pl.ds(0, SIDE - 1)
    half_rows = pl.ds(0, ROWS // 2)
    for index, (weight, mine) in enumerate(((proj_a, y), (proj_b, z))):
        wait_for(weight.at[three, half_rows], proj_recv.at[index])
        for s in line:
            piece = weight.at[(mine + s) % SIDE, core_rows]
            remote(piece, piece, relay_send.at[index], relay_recv.at[index], partner, "dp")

    loads[0].wait()
    wait_for(proj_a.at[three, half_rows], relay_recv.at[0])
    for i in range(SIDE):
        quarter = (z + 1 + i) % SIDE
        wait_for(oa.at[0, :, pl.ds(0, 3 * HEAD)], oa_recv.at[quarter])
        left = oa[quarter]
        for q in range(2):
            for n in range(2):
                c = slice(q * CHUNK + n * TILE, q * CHUNK + (n + 1) * TILE)
                right = proj_a[:, :, c].reshape(512, TILE)
                part_a[q, quarter, :, n * TILE:(n + 1) * TILE] = dot(left, right).astype(jnp.bfloat16)
        if i < SIDE - 1:
            remote(part_a.at[0, quarter], sum_a.at[0, z], r_send.at[0], ra_recv.at[0], quarter * SIDE + y)
    for s in (1, 2, 3):
        peer_z = (z + s) % SIDE
        remote(part_a.at[1, peer_z], sum_a.at[1, z], r_send.at[0], ra_recv.at[1], peer_z * SIDE + y)
    loads[1].wait()
    wait_for(proj_b.at[three, half_rows], relay_recv.at[1])
    wait_for(ob.at[:, :, pl.ds(0, 3 * HEAD)], ob_recv)
    for q in range(2):
        @pl.loop(0, 2)
        def _(n):
            c = pl.ds(pl.multiple_of(q * CHUNK + n * TILE, TILE), TILE)
            right = proj_b[:, :, c].reshape(512, TILE)
            block = dot(ob[...].reshape(512, 512), right).astype(jnp.bfloat16)
            part_b[q, :, :, pl.ds(pl.multiple_of(n * TILE, TILE), TILE)] = block.reshape(SIDE, ROWS, TILE)

        for s in line:
            peer_y = (y + s) % SIDE
            remote(part_b.at[q, peer_y], sum_b.at[q, y], r_send.at[1], rb_recv.at[q], z * SIDE + peer_y)
    for q in range(2):
        sum_a[q, z] = part_a[q, z]
        sum_b[q, y] = part_b[q, y]

    pieces = ((sum_a, ra_recv, 0, 0), (sum_b, rb_recv, 0, HALF),
              (sum_a, ra_recv, 1, CHUNK), (sum_b, rb_recv, 1, HALF + CHUNK))
    loads[2].wait()
    for k, (sums, recv, q, start) in enumerate(pieces):
        wait_for(sums.at[q, three], recv.at[q])
        total = res[:, start:start + CHUNK].astype(jnp.float32)
        for i in range(SIDE):
            total = total + sums[q, i].astype(jnp.float32)
        stream = total.astype(jnp.bfloat16)
        acc[:, start:start + CHUNK] = stream.astype(jnp.float32)
        for n in range(2):
            c = slice(n * TILE, (n + 1) * TILE)
            rows = dot(pick[...], stream[:, c]).astype(jnp.bfloat16)
            xs[k, :, :, c] = rows.reshape(N_SP, CAP, TILE)
        for i, (a, b) in enumerate(SHIFTS):
            if i != OWN:
                sem = d_recv.at[k] if k < CHUNKS - 1 else d_recv.at[k + i // PER_GROUP]
                remote(xs.at[k, i], xr.at[k, i], d_send, sem, at(a, b))
        xr[k, OWN] = xs[k, OWN]

    for load in loads[3:]:
        load.wait()
    fifteen = pl.ds(0, N_SP - 1)
    for k in range(CHUNKS - 1):
        start = pieces[k][3]
        wait_for(xr.at[k, fifteen], d_recv.at[k])

        @pl.loop(0, N_SP // 2)
        def _(i):
            rows = xr[k, pl.ds(2 * i, 2)].astype(jnp.float32).reshape(2 * CAP, CHUNK)
            r = pl.ds(pl.multiple_of(i * 2 * CAP, 2 * CAP), 2 * CAP)
            scaled[r, :] = (rows * gain_ref[:, start:start + CHUNK]).astype(jnp.bfloat16)
            square = jnp.sum(rows * rows, axis=-1, keepdims=True)
            square = jnp.broadcast_to(square, (2 * CAP, HEAD))
            squares[r, :] = square if k == 0 else squares[r, :] + square

        @pl.loop(0, FFE // TILE)
        def _(n):
            c = pl.ds(pl.multiple_of(n * TILE, TILE), TILE)
            for weight, total in ((wg, gate_acc), (wu, up_acc)):
                new = dot(scaled[...], weight[start:start + CHUNK, c])
                total[:, c] = new if k == 0 else total[:, c] + new

    def remote_count(g):
        return PER_GROUP - (1 if OWN // PER_GROUP == g else 0)

    last = CHUNKS - 1
    start = pieces[last][3]
    for g in range(GROUPS):
        mine = slice(g * PER_GROUP, (g + 1) * PER_GROUP)
        lines = slice(g * GROUP_ROWS, (g + 1) * GROUP_ROWS)
        wait_for(xr.at[last, pl.ds(g * PER_GROUP, remote_count(g))], d_recv.at[last + g])
        rows = xr[last, mine].astype(jnp.float32).reshape(GROUP_ROWS, CHUNK)
        scaled[lines, :] = (rows * gain_ref[:, start:start + CHUNK]).astype(jnp.bfloat16)
        square = squares[lines, 0:1] + jnp.sum(rows * rows, axis=-1, keepdims=True)
        factor = lax.rsqrt(square * (1.0 / WIDTH) + EPS)
        squares[lines, :] = jnp.broadcast_to(factor, (GROUP_ROWS, HEAD))

        @pl.loop(0, FFE // TILE)
        def _(n):
            c = pl.ds(pl.multiple_of(n * TILE, TILE), TILE)
            x = scaled[lines, :]
            norm = jnp.concatenate([squares[lines, :], squares[lines, :]], axis=1)
            gate = (gate_acc[lines, c] + dot(x, wg[start:start + CHUNK, c])) * norm
            upper = (up_acc[lines, c] + dot(x, wu[start:start + CHUNK, c])) * norm
            hid[:, c] = (gate / (1.0 + jnp.exp(-gate)) * upper).astype(jnp.bfloat16)

        @pl.loop(0, WIDTH // 512)
        def _(n):
            c = pl.ds(pl.multiple_of(n * 512, 512), 512)
            result = dot(hid[...], wd[:, c]).astype(jnp.bfloat16)
            ys[mine, :, c] = result.reshape(PER_GROUP, CAP, 512)

        for i in range(g * PER_GROUP, (g + 1) * PER_GROUP):
            if i == OWN:
                yr[i] = ys[i]
            else:
                a, b = SHIFTS[i]
                remote(ys.at[i], yr.at[i], y_send, y_recv.at[g], at(-a, -b))

    for g in range(GROUPS):
        wait_for(yr.at[pl.ds(g * PER_GROUP, remote_count(g))], y_recv.at[g])

        @pl.loop(0, WIDTH // 512)
        def _(n):
            c = pl.ds(pl.multiple_of(n * 512, 512), 512)
            lanes = slice(g * GROUP_ROWS, (g + 1) * GROUP_ROWS)
            got = yr[g * PER_GROUP:(g + 1) * PER_GROUP, :, c].reshape(GROUP_ROWS, 512)
            total = acc[:, c] + dot(mix_hi[:, lanes], got) + dot(mix_lo[:, lanes], got)
            if g < GROUPS - 1:
                acc[:, c] = total
            else:
                out_ref[0, :, c] = total.astype(jnp.bfloat16)

    for t, (src, dst) in enumerate(heads):
        wait_for(dst.at[pl.ds(0, ROWS * (N_SP - 1))], head_send.at[t])
    for i in range(2):
        wait_for(proj_a.at[three, half_rows], proj_send.at[i])
        wait_for(proj_a.at[three, half_rows], relay_send.at[i])
        wait_for(o_buf.at[three], o_send.at[i])
        wait_for(part_a.at[:, three], r_send.at[i])
    wait_for(xs.at[:, fifteen], d_send)
    wait_for(ys.at[fifteen], y_send)


def body(
    queries, keys, values, proj_weight, residual, norm_gain, route, route_weight,
    w_gate, w_up, w_down,
):
    bf16, f32 = jnp.bfloat16, jnp.float32
    vmem = pltpu.VMEM
    dma = pltpu.SemaphoreType.DMA
    anywhere = pl.BlockSpec(memory_space=pl.ANY)
    inside = pl.BlockSpec(memory_space=pltpu.VMEM)
    scratch = [
        vmem((LENGTH, HEAD), bf16), vmem((LENGTH, HEAD), bf16), vmem((LENGTH, HEAD), bf16),
        vmem((LENGTH, LENGTH), bf16), vmem((LENGTH, HEAD), f32), vmem((TILE, TILE + HEAD), bf16),
        vmem((SIDE, SIDE, ROWS, HEAD), bf16),
        vmem((SIDE, ROWS, 512), bf16), vmem((SIDE, ROWS, 512), bf16),
        vmem((SIDE, ROWS, HALF), bf16), vmem((SIDE, ROWS, HALF), bf16),
        vmem((2, SIDE, ROWS, CHUNK), bf16), vmem((2, SIDE, ROWS, CHUNK), bf16),
        vmem((2, SIDE, ROWS, CHUNK), bf16), vmem((2, SIDE, ROWS, CHUNK), bf16),
        vmem((ROWS, WIDTH), bf16), vmem((ROWS, WIDTH), f32),
        vmem((N_SP * CAP, ROWS), bf16), vmem((ROWS, N_SP * CAP), bf16), vmem((ROWS, N_SP * CAP), bf16),
        vmem((CHUNKS, N_SP, CAP, CHUNK), bf16), vmem((CHUNKS, N_SP, CAP, CHUNK), bf16),
        vmem((N_SP, CAP, WIDTH), bf16), vmem((N_SP, CAP, WIDTH), bf16),
        vmem((N_SP * CAP, CHUNK), bf16), vmem((N_SP * CAP, HEAD), f32),
        vmem((N_SP * CAP, FFE), f32), vmem((N_SP * CAP, FFE), f32),
        vmem((GROUP_ROWS, FFE), bf16),
        vmem((WIDTH, FFE), bf16), vmem((WIDTH, FFE), bf16), vmem((FFE, WIDTH), bf16),
        dma((6,)), dma((3,)), dma((3,)), dma((2,)), dma((2,)), dma((2,)), dma((2,)),
        dma((2,)), dma((SIDE,)), dma, dma((2,)), dma((2,)), dma((2,)),
        dma, dma((CHUNKS - 1 + GROUPS,)), dma, dma((GROUPS,)),
    ]
    return pl.pallas_call(
        body_kernel,
        out_shape=jax.ShapeDtypeStruct((1, ROWS, WIDTH), bf16),
        in_specs=[anywhere] * 5 + [inside] * 3 + [anywhere] * 3,
        out_specs=inside,
        scratch_shapes=scratch,
        compiler_params=pltpu.CompilerParams(
            collective_id=0, has_side_effects=True, vmem_limit_bytes=56 * 1024 * 1024
        ),
        name="layer",
    )(
        queries, keys, values, proj_weight, residual, norm_gain.reshape(1, WIDTH),
        jnp.swapaxes(route, 1, 2), jnp.swapaxes(route_weight, 1, 2), w_gate, w_up, w_down,
    )


def solution(mesh):
    return jax.shard_map(
        body,
        mesh=mesh,
        in_specs=(
            P("dp", "sp", None),
            P("dp", "sp", None),
            P("dp", "sp", None),
            P("sp", None),
            P("dp", "sp", None),
            P(),
            P("dp", "sp", None),
            P("dp", "sp", None),
            P("sp", None, None),
            P("sp", None, None),
            P("sp", None, None),
        ),
        out_specs=P("dp", "sp", None),
        check_vma=False,
    )
```

time: 121 us -> 115 us (0.950)
  Pallas kernels: 116 us -> 112 us
  local copies, waits for them, and re-layouts: 4.7 us -> 1.88 us
    pallas_call x1, Pallas kernels: 116 us -> 112 us  [body(): pl.pallas_call(body_kernel, out_shape=jax.ShapeDtypeStruct((1, ROWS, WIDT...]
    unnamed x3 -> x1, local copies, waits for them, and re-layouts: 4.7 us -> 1.88 us
where the time goes in v2:
time: 115 us; the launch traced here: 114 us
  Pallas kernels  112 us (97%)
  local copies, waits for them, and re-layouts  1.88 us (2%)
    pallas_call x1, Pallas kernels, body(): pl.pallas_call(body_kernel, out_shape=jax.ShapeDtypeStruct((1, ROWS, WIDT...  112 us

profile of v2, /device:TPU:0, one launch (start us, length us, event | category | flops | bytes accessed | tf_op | source)
XLA Modules:
  0.0 113.8 jit_solution(5583424184373593336)
XLA Ops:
  0.0 111.9 %layer.1 = bf16[1,128,2048]{2,1,0:T(8,128)(2,1)} custom-call(bf16[1,128,2048]{2,1,0:T(8,128)(2,1)} %q_hbm.1, bf16[1,128,2048]{2,1,0:T(8,128)(2,1)} %k_hbm.1, bf16[1,128,2048]{2,1,0:T(8,128)(2,1)} %v_hbm.1, bf16[128,2048]{1,0:T(8,128)(2,1)} %proj_hbm.1, bf16[1,128,2048]{2,1,0:T(8,128)(2,1)} %res_hbm.1, f32[1,2048]{1,0:T(1,128)} %bitcast.3, ...), custom_call_target="tpu_custom_call" | custom-call | tf_op jit(solution)/shard_map/layer/pallas_call | solution.py:397
  112.0 1.9 %copy.13 = bf16[1,128,2048]{2,1,0:T(8,128)(2,1)} copy(bf16[1,128,2048]{2,1,0:T(8,128)(2,1)} %layer.1) | data formatting | bytes 1048576

commit v3 on v2

--- a/solution.py
+++ b/solution.py
@@ -184,27 +184,19 @@
         w_att[q_rows, k_rows] = weight.astype(jnp.bfloat16)
         carry[q_rows, :] = total
 
-    @pl.loop(0, 4)
-    def _(i):
-        for half in range(2):
-            base = pl.multiple_of(i * 512 + half * TILE, TILE)
-            weights(base, base, True)
-
-    @pl.loop(0, 2)
-    def _(i):
-        for half in range(2):
-            base = pl.multiple_of(i * 1024 + half * 512, TILE)
-            weights(base + TILE, base, False)
-
-    for big in range(1, 4):
-        @pl.loop(0, 2 * big)
+    def quarter_weights(quarter):
+        base = pl.multiple_of(quarter * 512, 512)
+        weights(pl.multiple_of(base + TILE, TILE), pl.multiple_of(base + TILE, TILE), True)
+        weights(base, base, True)
+        weights(pl.multiple_of(base + TILE, TILE), base, False)
+
+        @pl.loop(0, 2 * quarter)
         def _(i):
-            k0 = pl.multiple_of((2 * big - 1 - i) * TILE, TILE)
+            k0 = pl.multiple_of((2 * quarter - 1 - i) * TILE, TILE)
             for half in range(2):
-                weights(big * 512 + half * TILE, k0, False)
-
-    wait_for(vh, head_recv.at[2])
-    for i in range(SIDE):
+                weights(pl.multiple_of(base + half * TILE, TILE), k0, False)
+
+    def quarter_values(i):
         quarter = (z + 1 + i) % SIDE
         rows = pl.ds(pl.multiple_of(quarter * 512, 512), 512)
         o_buf[quarter] = dot(w_att[rows, :], vh[...]).astype(jnp.bfloat16).reshape(SIDE, ROWS, HEAD)
@@ -217,6 +209,16 @@
             remote(o_buf.at[quarter, peer_y], oa.at[quarter, :, cols(y)], o_send.at[0],
                    oa_recv.at[quarter], z * SIDE + peer_y)
         oa[quarter, :, cols(y)] = o_buf[quarter, y]
+
+    quarter_weights((z + 1) % SIDE)
+    quarter_weights((z + 2) % SIDE)
+    wait_for(vh, head_recv.at[2])
+    quarter_values(0)
+    quarter_values(1)
+    quarter_weights((z + 3) % SIDE)
+    quarter_values(2)
+    quarter_weights(z)
+    quarter_values(3)
 
     three = pl.ds(0, SIDE - 1)
     half_rows = pl.ds(0, ROWS // 2)
@@ -316,22 +318,19 @@
         scaled[lines, :] = (rows * gain_ref[:, start:start + CHUNK]).astype(jnp.bfloat16)
         square = squares[lines, 0:1] + jnp.sum(rows * rows, axis=-1, keepdims=True)
         factor = lax.rsqrt(square * (1.0 / WIDTH) + EPS)
-        squares[lines, :] = jnp.broadcast_to(factor, (GROUP_ROWS, HEAD))
-
-        @pl.loop(0, FFE // TILE)
-        def _(n):
-            c = pl.ds(pl.multiple_of(n * TILE, TILE), TILE)
+
+        norm = jnp.broadcast_to(factor, (GROUP_ROWS, TILE))
+        for n in range(FFE // TILE):
+            c = slice(n * TILE, (n + 1) * TILE)
             x = scaled[lines, :]
-            norm = jnp.concatenate([squares[lines, :], squares[lines, :]], axis=1)
             gate = (gate_acc[lines, c] + dot(x, wg[start:start + CHUNK, c])) * norm
             upper = (up_acc[lines, c] + dot(x, wu[start:start + CHUNK, c])) * norm
             hid[:, c] = (gate / (1.0 + jnp.exp(-gate)) * upper).astype(jnp.bfloat16)
 
-        @pl.loop(0, WIDTH // 512)
-        def _(n):
-            c = pl.ds(pl.multiple_of(n * 512, 512), 512)
+        for n in range(WIDTH // TILE):
+            c = slice(n * TILE, (n + 1) * TILE)
             result = dot(hid[...], wd[:, c]).astype(jnp.bfloat16)
-            ys[mine, :, c] = result.reshape(PER_GROUP, CAP, 512)
+            ys[mine, :, c] = result.reshape(PER_GROUP, CAP, TILE)
 
         for i in range(g * PER_GROUP, (g + 1) * PER_GROUP):
             if i == OWN:
@@ -343,9 +342,8 @@
     for g in range(GROUPS):
         wait_for(yr.at[pl.ds(g * PER_GROUP, remote_count(g))], y_recv.at[g])
 
-        @pl.loop(0, WIDTH // 512)
-        def _(n):
-            c = pl.ds(pl.multiple_of(n * 512, 512), 512)
+        for n in range(WIDTH // 512):
+            c = slice(n * 512, (n + 1) * 512)
             lanes = slice(g * GROUP_ROWS, (g + 1) * GROUP_ROWS)
             got = yr[g * PER_GROUP:(g + 1) * PER_GROUP, :, c].reshape(GROUP_ROWS, 512)
             total = acc[:, c] + dot(mix_hi[:, lanes], got) + dot(mix_lo[:, lanes], got)

time: 115 us -> 111 us (0.965)
  Pallas kernels: 112 us -> 108 us
    pallas_call x1, Pallas kernels: 112 us -> 108 us  [body(): pl.pallas_call(body_kernel, out_shape=jax.ShapeDtypeStruct((1, ROWS, WIDT...]
where the time goes in v3:
time: 111 us; the launch traced here: 110 us
  Pallas kernels  108 us (97%)
  local copies, waits for them, and re-layouts  1.88 us (2%)
    pallas_call x1, Pallas kernels, body(): pl.pallas_call(body_kernel, out_shape=jax.ShapeDtypeStruct((1, ROWS, WIDT...  108 us

profile of v3, /device:TPU:0, one launch (start us, length us, event | category | flops | bytes accessed | tf_op | source)
XLA Modules:
  0.0 110.2 jit_solution(5811261240822222417)
XLA Ops:
  0.0 108.3 %layer.1 = bf16[1,128,2048]{2,1,0:T(8,128)(2,1)} custom-call(bf16[1,128,2048]{2,1,0:T(8,128)(2,1)} %q_hbm.1, bf16[1,128,2048]{2,1,0:T(8,128)(2,1)} %k_hbm.1, bf16[1,128,2048]{2,1,0:T(8,128)(2,1)} %v_hbm.1, bf16[128,2048]{1,0:T(8,128)(2,1)} %proj_hbm.1, bf16[1,128,2048]{2,1,0:T(8,128)(2,1)} %res_hbm.1, f32[1,2048]{1,0:T(1,128)} %bitcast.3, ...), custom_call_target="tpu_custom_call" | custom-call | tf_op jit(solution)/shard_map/layer/pallas_call | solution.py:395
  108.3 1.9 %copy.13 = bf16[1,128,2048]{2,1,0:T(8,128)(2,1)} copy(bf16[1,128,2048]{2,1,0:T(8,128)(2,1)} %layer.1) | data formatting | bytes 1048576

commit v4 on v3

--- a/solution.py
+++ b/solution.py
@@ -44,7 +44,7 @@
     q_hbm, k_hbm, v_hbm, proj_hbm, res_hbm, gain_ref, route_ref, rw_ref,
     wg_hbm, wu_hbm, wd_hbm,
     out_ref,
-    qh, kh, vh, w_att, carry, tri, o_buf, oa, ob, proj_a, proj_b,
+    qh, kh, vh, w_att, carry, softer, power, tri, o_buf, oa, ob, proj_a, proj_b,
     part_a, part_b, sum_a, sum_b, res, acc, pick, mix_hi, mix_lo,
     xs, xr, ys, yr, scaled, squares, gate_acc, up_acc, hid, wg, wu, wd,
     local_sem, head_send, head_recv, proj_send, proj_recv, relay_send, relay_recv,
@@ -155,46 +155,60 @@
 
     wait_for(kh, head_recv.at[0])
     wait_for(qh, head_recv.at[1])
-    scale = HEAD ** (-0.5) * LOG2E
-
-    def weights(q0, k0, diagonal):
-        q_rows = pl.ds(q0, TILE)
-        k_rows = pl.ds(k0, TILE)
+    scale = HEAD ** (-0.5)
+
+    causal = lax.broadcasted_iota(jnp.int32, (TILE, TILE), 1) < lax.broadcasted_iota(
+        jnp.int32, (TILE, TILE), 0
+    )
+
+    def soften(base, lines, k0, which, diagonal):
+        rows = slice(*lines)
         u = lax.dot_general(
-            qh[q_rows, :], kh[k_rows, :], (((1,), (1,)), ((), ())),
+            qh[pl.ds(pl.multiple_of(base + lines[0], TILE), lines[1] - lines[0]), :],
+            kh[pl.ds(k0, TILE), :], (((1,), (1,)), ((), ())),
             preferred_element_type=jnp.float32,
         ) * scale
-        low = jnp.log(1.0 + jnp.exp2(-jnp.abs(u))) * LOG2E
+        low = jnp.log(1.0 + jnp.exp2(jnp.abs(u) * -LOG2E))
         soft = jnp.maximum(u, 0.0) + low
         if diagonal:
-            causal = lax.broadcasted_iota(jnp.int32, (TILE, TILE), 1) < lax.broadcasted_iota(
-                jnp.int32, (TILE, TILE), 0
-            )
             soft = jnp.where(causal, soft, 0.0)
-        sums = dot(soft.astype(jnp.bfloat16), tri[...])
-        power = jnp.minimum(u, 0.0) - low - sums[:, :TILE]
+        softer[which, rows, :] = soft.astype(jnp.bfloat16)
+        power[which, rows, :] = jnp.minimum(u, 0.0) - low
+
+    def weigh(base, lines, k0, which, diagonal, fresh):
+        rows = slice(*lines)
+        sums = dot(softer[which, rows, :], tri[...])
+        less = sums[:, :TILE]
         total = sums[:, TILE:]
-        if not diagonal:
-            later = carry[q_rows, :]
-            power = power - jnp.concatenate([later, later], axis=1)
+        if not fresh:
+            later = carry[rows, :]
+            less = less + jnp.concatenate([later, later], axis=1)
             total = total + later
-        weight = jnp.exp2(power)
+        weight = jnp.exp2((power[which, rows, :] - less) * LOG2E)
         if diagonal:
             weight = jnp.where(causal, weight, 0.0)
-        w_att[q_rows, k_rows] = weight.astype(jnp.bfloat16)
-        carry[q_rows, :] = total
+        place = pl.ds(pl.multiple_of(base + lines[0], TILE), lines[1] - lines[0])
+        w_att[place, pl.ds(k0, TILE)] = weight.astype(jnp.bfloat16)
+        carry[rows, :] = total
+
+    upper, lower, both = (0, TILE), (TILE, 2 * TILE), (0, 2 * TILE)
 
     def quarter_weights(quarter):
         base = pl.multiple_of(quarter * 512, 512)
-        weights(pl.multiple_of(base + TILE, TILE), pl.multiple_of(base + TILE, TILE), True)
-        weights(base, base, True)
-        weights(pl.multiple_of(base + TILE, TILE), base, False)
-
-        @pl.loop(0, 2 * quarter)
+        second = pl.multiple_of(base + TILE, TILE)
+        soften(base, lower, second, 1, True)
+        soften(base, upper, base, 0, True)
+        soften(base, lower, base, 0, False)
+        weigh(base, lower, second, 1, True, True)
+        weigh(base, upper, base, 0, True, True)
+        weigh(base, lower, base, 0, False, False)
+
+        @pl.loop(0, quarter)
         def _(i):
-            k0 = pl.multiple_of((2 * quarter - 1 - i) * TILE, TILE)
-            for half in range(2):
-                weights(pl.multiple_of(base + half * TILE, TILE), k0, False)
+            for which in range(2):
+                k0 = pl.multiple_of((2 * quarter - 2 * i - 1 - which) * TILE, TILE)
+                soften(base, both, k0, which, False)
+                weigh(base, both, k0, which, False, False)
 
     def quarter_values(i):
         quarter = (z + 1 + i) % SIDE
@@ -210,27 +224,17 @@
                    oa_recv.at[quarter], z * SIDE + peer_y)
         oa[quarter, :, cols(y)] = o_buf[quarter, y]
 
-    quarter_weights((z + 1) % SIDE)
-    quarter_weights((z + 2) % SIDE)
-    wait_for(vh, head_recv.at[2])
-    quarter_values(0)
-    quarter_values(1)
-    quarter_weights((z + 3) % SIDE)
-    quarter_values(2)
-    quarter_weights(z)
-    quarter_values(3)
-
     three = pl.ds(0, SIDE - 1)
     half_rows = pl.ds(0, ROWS // 2)
-    for index, (weight, mine) in enumerate(((proj_a, y), (proj_b, z))):
-        wait_for(weight.at[three, half_rows], proj_recv.at[index])
-        for s in line:
-            piece = weight.at[(mine + s) % SIDE, core_rows]
-            remote(piece, piece, relay_send.at[index], relay_recv.at[index], partner, "dp")
-
-    loads[0].wait()
-    wait_for(proj_a.at[three, half_rows], relay_recv.at[0])
-    for i in range(SIDE):
+
+    def relay():
+        for index, (weight, mine) in enumerate(((proj_a, y), (proj_b, z))):
+            wait_for(weight.at[three, half_rows], proj_recv.at[index])
+            for s in line:
+                piece = weight.at[(mine + s) % SIDE, core_rows]
+                remote(piece, piece, relay_send.at[index], relay_recv.at[index], partner, "dp")
+
+    def project_z(i):
         quarter = (z + 1 + i) % SIDE
         wait_for(oa.at[0, :, pl.ds(0, 3 * HEAD)], oa_recv.at[quarter])
         left = oa[quarter]
@@ -239,15 +243,10 @@
                 c = slice(q * CHUNK + n * TILE, q * CHUNK + (n + 1) * TILE)
                 right = proj_a[:, :, c].reshape(512, TILE)
                 part_a[q, quarter, :, n * TILE:(n + 1) * TILE] = dot(left, right).astype(jnp.bfloat16)
-        if i < SIDE - 1:
-            remote(part_a.at[0, quarter], sum_a.at[0, z], r_send.at[0], ra_recv.at[0], quarter * SIDE + y)
-    for s in (1, 2, 3):
-        peer_z = (z + s) % SIDE
-        remote(part_a.at[1, peer_z], sum_a.at[1, z], r_send.at[0], ra_recv.at[1], peer_z * SIDE + y)
-    loads[1].wait()
-    wait_for(proj_b.at[three, half_rows], relay_recv.at[1])
-    wait_for(ob.at[:, :, pl.ds(0, 3 * HEAD)], ob_recv)
-    for q in range(2):
+            if i < SIDE - 1:
+                remote(part_a.at[q, quarter], sum_a.at[q, z], r_send.at[0], ra_recv.at[q], quarter * SIDE + y)
+
+    def project_y(q):
         @pl.loop(0, 2)
         def _(n):
             c = pl.ds(pl.multiple_of(q * CHUNK + n * TILE, TILE), TILE)
@@ -258,6 +257,28 @@
         for s in line:
             peer_y = (y + s) % SIDE
             remote(part_b.at[q, peer_y], sum_b.at[q, y], r_send.at[1], rb_recv.at[q], z * SIDE + peer_y)
+
+    quarter_weights((z + 1) % SIDE)
+    quarter_weights((z + 2) % SIDE)
+    wait_for(vh, head_recv.at[2])
+    quarter_values(0)
+    quarter_values(1)
+    quarter_weights((z + 3) % SIDE)
+    quarter_values(2)
+    relay()
+    loads[0].wait()
+    loads[1].wait()
+    wait_for(proj_a.at[three, half_rows], relay_recv.at[0])
+    project_z(0)
+    project_z(1)
+    quarter_weights(z)
+    quarter_values(3)
+    wait_for(proj_b.at[three, half_rows], relay_recv.at[1])
+    wait_for(ob.at[:, :, pl.ds(0, 3 * HEAD)], ob_recv)
+    project_y(0)
+    project_z(2)
+    project_y(1)
+    project_z(3)
     for q in range(2):
         sum_a[q, z] = part_a[q, z]
         sum_b[q, y] = part_b[q, y]
@@ -374,7 +395,8 @@
     inside = pl.BlockSpec(memory_space=pltpu.VMEM)
     scratch = [
         vmem((LENGTH, HEAD), bf16), vmem((LENGTH, HEAD), bf16), vmem((LENGTH, HEAD), bf16),
-        vmem((LENGTH, LENGTH), bf16), vmem((LENGTH, HEAD), f32), vmem((TILE, TILE + HEAD), bf16),
+        vmem((LENGTH, LENGTH), bf16), vmem((2 * TILE, HEAD), f32),
+        vmem((2, 2 * TILE, TILE), bf16), vmem((2, 2 * TILE, TILE), f32), vmem((TILE, TILE + HEAD), bf16),
         vmem((SIDE, SIDE, ROWS, HEAD), bf16),
         vmem((SIDE, ROWS, 512), bf16), vmem((SIDE, ROWS, 512), bf16),
         vmem((SIDE, ROWS, HALF), bf16), vmem((SIDE, ROWS, HALF), bf16),

time: 111 us -> 108 us (0.973)
  Pallas kernels: 108 us -> 105 us
    pallas_call x1, Pallas kernels: 108 us -> 105 us  [body(): pl.pallas_call(body_kernel, out_shape=jax.ShapeDtypeStruct((1, ROWS, WIDT...]
where the time goes in v4:
time: 108 us; the launch traced here: 106 us
  Pallas kernels  105 us (97%)
  local copies, waits for them, and re-layouts  1.88 us (2%)
    pallas_call x1, Pallas kernels, body(): pl.pallas_call(body_kernel, out_shape=jax.ShapeDtypeStruct((1, ROWS, WIDT...  105 us

profile of v4, /device:TPU:0, one launch (start us, length us, event | category | flops | bytes accessed | tf_op | source)
XLA Modules:
  0.0 106.5 jit_solution(816840180436190955)
XLA Ops:
  0.0 104.6 %layer.1 = bf16[1,128,2048]{2,1,0:T(8,128)(2,1)} custom-call(bf16[1,128,2048]{2,1,0:T(8,128)(2,1)} %q_hbm.1, bf16[1,128,2048]{2,1,0:T(8,128)(2,1)} %k_hbm.1, bf16[1,128,2048]{2,1,0:T(8,128)(2,1)} %v_hbm.1, bf16[128,2048]{1,0:T(8,128)(2,1)} %proj_hbm.1, bf16[1,128,2048]{2,1,0:T(8,128)(2,1)} %res_hbm.1, f32[1,2048]{1,0:T(1,128)} %bitcast.3, ...), custom_call_target="tpu_custom_call" | custom-call | tf_op jit(solution)/shard_map/layer/pallas_call | solution.py:417
  104.6 1.9 %copy.13 = bf16[1,128,2048]{2,1,0:T(8,128)(2,1)} copy(bf16[1,128,2048]{2,1,0:T(8,128)(2,1)} %layer.1) | data formatting | bytes 1048576

commit v5 on v4

--- a/solution.py
+++ b/solution.py
@@ -17,9 +17,10 @@
 LENGTH = 2048
 WIDTH = 2048
 FFE = 1024
-HALF = 1024
-CHUNK = 512
-CHUNKS = 4
+COLS_Z = 1024
+COLS_Y = WIDTH - COLS_Z
+PIECES = (("y", COLS_Z, 512), ("z", 0, 512), ("y", COLS_Z + 512, 512), ("z", 512, 512))
+EARLY = 2
 CAP = 32
 TILE = 256
 LOG2E = 1.0 / math.log(2.0)
@@ -45,11 +46,13 @@
     wg_hbm, wu_hbm, wd_hbm,
     out_ref,
     qh, kh, vh, w_att, carry, softer, power, tri, o_buf, oa, ob, proj_a, proj_b,
-    part_a, part_b, sum_a, sum_b, res, acc, pick, mix_hi, mix_lo,
-    xs, xr, ys, yr, scaled, squares, gate_acc, up_acc, hid, wg, wu, wd,
+    part0, part1, part2, part3, sum0, sum1, sum2, sum3, res, acc, pick, mix_hi, mix_lo,
+    xs0, xs1, xs2, xs3, xr0, xr1, xr2, xr3, ys, yr, scaled, squares, gate_acc, up_acc, hid, wg, wu, wd,
     local_sem, head_send, head_recv, proj_send, proj_recv, relay_send, relay_recv,
-    o_send, oa_recv, ob_recv, r_send, ra_recv, rb_recv, d_send, d_recv, y_send, y_recv,
+    o_send, oa_recv, ob_recv, r_send, r_recv, d_send, d_recv, group_recv, y_send, y_recv,
 ):
+    parts, sums = (part0, part1, part2, part3), (sum0, sum1, sum2, sum3)
+    xs, xr = (xs0, xs1, xs2, xs3), (xr0, xr1, xr2, xr3)
     me = lax.axis_index("sp")
     dp = lax.axis_index("dp")
     z = me // SIDE
@@ -92,8 +95,8 @@
     for t, (src, dst) in enumerate(heads):
         local(src.at[0, :, cols(me)], dst.at[my_rows], head_recv.at[t])
     loads = [
-        local(proj_hbm.at[:, pl.ds(0, HALF)], proj_a.at[y], local_sem.at[4]),
-        local(proj_hbm.at[:, pl.ds(HALF, HALF)], proj_b.at[z], local_sem.at[5]),
+        local(proj_hbm.at[:, pl.ds(0, COLS_Z)], proj_a.at[y], local_sem.at[4]),
+        local(proj_hbm.at[:, pl.ds(COLS_Z, COLS_Y)], proj_b.at[z], local_sem.at[5]),
     ]
 
     pl.semaphore_wait(barrier, N_SP)
@@ -103,16 +106,14 @@
         peer = at(a, b)
         remote(src.at[0, :, cols(peer)], dst.at[my_rows], head_send.at[t], head_recv.at[t], peer)
 
-    for a, b in others:
-        send_heads(0, a, b)
-        send_heads(1, a, b)
-    for a, b in others:
-        send_heads(2, a, b)
+    for t in range(3):
+        for a, b in others:
+            send_heads(t, a, b)
     for s in line:
-        remote(proj_hbm.at[core_rows, pl.ds(0, HALF)], proj_a.at[y, core_rows],
+        remote(proj_hbm.at[core_rows, pl.ds(0, COLS_Z)], proj_a.at[y, core_rows],
                proj_send.at[0], proj_recv.at[0], at(0, s))
     for s in line:
-        remote(proj_hbm.at[core_rows, pl.ds(HALF, HALF)], proj_b.at[z, core_rows],
+        remote(proj_hbm.at[core_rows, pl.ds(COLS_Z, COLS_Y)], proj_b.at[z, core_rows],
                proj_send.at[1], proj_recv.at[1], at(s, 0))
     loads += [
         local(res_hbm.at[0], res, local_sem.at[0]),
@@ -238,25 +239,27 @@
         quarter = (z + 1 + i) % SIDE
         wait_for(oa.at[0, :, pl.ds(0, 3 * HEAD)], oa_recv.at[quarter])
         left = oa[quarter]
-        for q in range(2):
-            for n in range(2):
-                c = slice(q * CHUNK + n * TILE, q * CHUNK + (n + 1) * TILE)
-                right = proj_a[:, :, c].reshape(512, TILE)
-                part_a[q, quarter, :, n * TILE:(n + 1) * TILE] = dot(left, right).astype(jnp.bfloat16)
+        for k, (axis, start, width) in enumerate(PIECES):
+            if axis == "y":
+                continue
+            for n in range(width // TILE):
+                right = proj_a[:, :, start + n * TILE:start + (n + 1) * TILE].reshape(512, TILE)
+                parts[k][quarter, :, n * TILE:(n + 1) * TILE] = dot(left, right).astype(jnp.bfloat16)
             if i < SIDE - 1:
-                remote(part_a.at[q, quarter], sum_a.at[q, z], r_send.at[0], ra_recv.at[q], quarter * SIDE + y)
-
-    def project_y(q):
-        @pl.loop(0, 2)
-        def _(n):
-            c = pl.ds(pl.multiple_of(q * CHUNK + n * TILE, TILE), TILE)
-            right = proj_b[:, :, c].reshape(512, TILE)
+                remote(parts[k].at[quarter], sums[k].at[z], r_send.at[k], r_recv.at[k], quarter * SIDE + y)
+            else:
+                sums[k][z] = parts[k][z]
+
+    def project_y(k):
+        start, width = PIECES[k][1] - COLS_Z, PIECES[k][2]
+        for n in range(width // TILE):
+            right = proj_b[:, :, start + n * TILE:start + (n + 1) * TILE].reshape(512, TILE)
             block = dot(ob[...].reshape(512, 512), right).astype(jnp.bfloat16)
-            part_b[q, :, :, pl.ds(pl.multiple_of(n * TILE, TILE), TILE)] = block.reshape(SIDE, ROWS, TILE)
-
+            parts[k][:, :, n * TILE:(n + 1) * TILE] = block.reshape(SIDE, ROWS, TILE)
         for s in line:
             peer_y = (y + s) % SIDE
-            remote(part_b.at[q, peer_y], sum_b.at[q, y], r_send.at[1], rb_recv.at[q], z * SIDE + peer_y)
+            remote(parts[k].at[peer_y], sums[k].at[y], r_send.at[k], r_recv.at[k], z * SIDE + peer_y)
+        sums[k][y] = parts[k][y]
 
     quarter_weights((z + 1) % SIDE)
     quarter_weights((z + 2) % SIDE)
@@ -266,86 +269,100 @@
     quarter_weights((z + 3) % SIDE)
     quarter_values(2)
     relay()
+    quarter_weights(z)
+    quarter_values(3)
     loads[0].wait()
     loads[1].wait()
-    wait_for(proj_a.at[three, half_rows], relay_recv.at[0])
-    project_z(0)
-    project_z(1)
-    quarter_weights(z)
-    quarter_values(3)
     wait_for(proj_b.at[three, half_rows], relay_recv.at[1])
     wait_for(ob.at[:, :, pl.ds(0, 3 * HEAD)], ob_recv)
     project_y(0)
+    wait_for(proj_a.at[three, half_rows], relay_recv.at[0])
+    project_z(0)
+    project_y(2)
+    project_z(1)
     project_z(2)
-    project_y(1)
     project_z(3)
-    for q in range(2):
-        sum_a[q, z] = part_a[q, z]
-        sum_b[q, y] = part_b[q, y]
-
-    pieces = ((sum_a, ra_recv, 0, 0), (sum_b, rb_recv, 0, HALF),
-              (sum_a, ra_recv, 1, CHUNK), (sum_b, rb_recv, 1, HALF + CHUNK))
+
+    last = len(PIECES) - 1
+
+    def dispatch(k, g, sem):
+        for i in range(g * PER_GROUP, (g + 1) * PER_GROUP):
+            if i != OWN:
+                remote(xs[k].at[i], xr[k].at[i], d_send.at[k], sem, at(*SHIFTS[i]))
+
     loads[2].wait()
-    for k, (sums, recv, q, start) in enumerate(pieces):
-        wait_for(sums.at[q, three], recv.at[q])
-        total = res[:, start:start + CHUNK].astype(jnp.float32)
-        for i in range(SIDE):
-            total = total + sums[q, i].astype(jnp.float32)
-        stream = total.astype(jnp.bfloat16)
-        acc[:, start:start + CHUNK] = stream.astype(jnp.float32)
-        for n in range(2):
+    for k, (axis, start, width) in enumerate(PIECES):
+        wait_for(sums[k].at[three], r_recv.at[k])
+        for n in range(width // TILE):
             c = slice(n * TILE, (n + 1) * TILE)
-            rows = dot(pick[...], stream[:, c]).astype(jnp.bfloat16)
-            xs[k, :, :, c] = rows.reshape(N_SP, CAP, TILE)
-        for i, (a, b) in enumerate(SHIFTS):
-            if i != OWN:
-                sem = d_recv.at[k] if k < CHUNKS - 1 else d_recv.at[k + i // PER_GROUP]
-                remote(xs.at[k, i], xr.at[k, i], d_send, sem, at(a, b))
-        xr[k, OWN] = xs[k, OWN]
+            place = slice(start + n * TILE, start + (n + 1) * TILE)
+            total = res[:, place].astype(jnp.float32)
+            for i in range(SIDE):
+                total = total + sums[k][i, :, c].astype(jnp.float32)
+            stream = total.astype(jnp.bfloat16)
+            acc[:, place] = stream.astype(jnp.float32)
+            rows = dot(pick[...], stream).astype(jnp.bfloat16)
+            xs[k][:, :, c] = rows.reshape(N_SP, CAP, TILE)
+        if k < EARLY:
+            for g in range(GROUPS):
+                dispatch(k, g, d_recv.at[k])
+        xr[k][OWN] = xs[k][OWN]
+        if k == EARLY:
+            dispatch(k, 0, group_recv.at[k - EARLY, 0])
+    for g in range(GROUPS):
+        for k in range(EARLY, last + 1):
+            if g > 0 or k > EARLY:
+                dispatch(k, g, group_recv.at[k - EARLY, g])
 
     for load in loads[3:]:
         load.wait()
     fifteen = pl.ds(0, N_SP - 1)
-    for k in range(CHUNKS - 1):
-        start = pieces[k][3]
-        wait_for(xr.at[k, fifteen], d_recv.at[k])
-
-        @pl.loop(0, N_SP // 2)
-        def _(i):
-            rows = xr[k, pl.ds(2 * i, 2)].astype(jnp.float32).reshape(2 * CAP, CHUNK)
-            r = pl.ds(pl.multiple_of(i * 2 * CAP, 2 * CAP), 2 * CAP)
-            scaled[r, :] = (rows * gain_ref[:, start:start + CHUNK]).astype(jnp.bfloat16)
+    for k, (axis, start, width) in enumerate(PIECES[:EARLY]):
+        wait_for(xr[k].at[fifteen], d_recv.at[k])
+
+        @pl.loop(0, GROUPS)
+        def _(g):
+            rows = xr[k][pl.ds(g * PER_GROUP, PER_GROUP)].astype(jnp.float32).reshape(GROUP_ROWS, width)
+            r = pl.ds(pl.multiple_of(g * GROUP_ROWS, GROUP_ROWS), GROUP_ROWS)
+            scaled[r, :width] = (rows * gain_ref[:, start:start + width]).astype(jnp.bfloat16)
             square = jnp.sum(rows * rows, axis=-1, keepdims=True)
-            square = jnp.broadcast_to(square, (2 * CAP, HEAD))
+            square = jnp.broadcast_to(square, (GROUP_ROWS, HEAD))
             squares[r, :] = square if k == 0 else squares[r, :] + square
 
-        @pl.loop(0, FFE // TILE)
+        @pl.loop(0, FFE // (2 * TILE))
         def _(n):
-            c = pl.ds(pl.multiple_of(n * TILE, TILE), TILE)
             for weight, total in ((wg, gate_acc), (wu, up_acc)):
-                new = dot(scaled[...], weight[start:start + CHUNK, c])
-                total[:, c] = new if k == 0 else total[:, c] + new
+                for half in range(2):
+                    c = pl.ds(pl.multiple_of(n * (2 * TILE) + half * TILE, TILE), TILE)
+                    new = dot(scaled[:, :width], weight[start:start + width, c])
+                    total[:, c] = new if k == 0 else total[:, c] + new
 
     def remote_count(g):
         return PER_GROUP - (1 if OWN // PER_GROUP == g else 0)
 
-    last = CHUNKS - 1
-    start = pieces[last][3]
     for g in range(GROUPS):
         mine = slice(g * PER_GROUP, (g + 1) * PER_GROUP)
         lines = slice(g * GROUP_ROWS, (g + 1) * GROUP_ROWS)
-        wait_for(xr.at[last, pl.ds(g * PER_GROUP, remote_count(g))], d_recv.at[last + g])
-        rows = xr[last, mine].astype(jnp.float32).reshape(GROUP_ROWS, CHUNK)
-        scaled[lines, :] = (rows * gain_ref[:, start:start + CHUNK]).astype(jnp.bfloat16)
-        square = squares[lines, 0:1] + jnp.sum(rows * rows, axis=-1, keepdims=True)
+        square = squares[lines, 0:1]
+        late = []
+        for k in range(EARLY, last + 1):
+            axis, start, width = PIECES[k]
+            wait_for(xr[k].at[pl.ds(g * PER_GROUP, remote_count(g))], group_recv.at[k - EARLY, g])
+            rows = xr[k][mine].astype(jnp.float32).reshape(GROUP_ROWS, width)
+            square = square + jnp.sum(rows * rows, axis=-1, keepdims=True)
+            at_col = (k - EARLY) * 512
+            scaled[lines, at_col:at_col + width] = (rows * gain_ref[:, start:start + width]).astype(jnp.bfloat16)
+            late.append((at_col, start, width))
         factor = lax.rsqrt(square * (1.0 / WIDTH) + EPS)
-
         norm = jnp.broadcast_to(factor, (GROUP_ROWS, TILE))
         for n in range(FFE // TILE):
             c = slice(n * TILE, (n + 1) * TILE)
-            x = scaled[lines, :]
-            gate = (gate_acc[lines, c] + dot(x, wg[start:start + CHUNK, c])) * norm
-            upper = (up_acc[lines, c] + dot(x, wu[start:start + CHUNK, c])) * norm
+            gate, upper = gate_acc[lines, c], up_acc[lines, c]
+            for at_col, start, width in late:
+                x = scaled[lines, at_col:at_col + width]
+                gate = gate + dot(x, wg[start:start + width, c])
+                upper = upper + dot(x, wu[start:start + width, c])
+            gate, upper = gate * norm, upper * norm
             hid[:, c] = (gate / (1.0 + jnp.exp(-gate)) * upper).astype(jnp.bfloat16)
 
         for n in range(WIDTH // TILE):
@@ -376,11 +393,13 @@
     for t, (src, dst) in enumerate(heads):
         wait_for(dst.at[pl.ds(0, ROWS * (N_SP - 1))], head_send.at[t])
     for i in range(2):
-        wait_for(proj_a.at[three, half_rows], proj_send.at[i])
-        wait_for(proj_a.at[three, half_rows], relay_send.at[i])
+        weight = (proj_a, proj_b)[i]
+        wait_for(weight.at[three, half_rows], proj_send.at[i])
+        wait_for(weight.at[three, half_rows], relay_send.at[i])
         wait_for(o_buf.at[three], o_send.at[i])
-        wait_for(part_a.at[:, three], r_send.at[i])
-    wait_for(xs.at[:, fifteen], d_send)
+    for k in range(len(PIECES)):
+        wait_for(parts[k].at[three], r_send.at[k])
+        wait_for(xs[k].at[fifteen], d_send.at[k])
     wait_for(ys.at[fifteen], y_send)
 
 
@@ -399,24 +418,27 @@
         vmem((2, 2 * TILE, TILE), bf16), vmem((2, 2 * TILE, TILE), f32), vmem((TILE, TILE + HEAD), bf16),
         vmem((SIDE, SIDE, ROWS, HEAD), bf16),
         vmem((SIDE, ROWS, 512), bf16), vmem((SIDE, ROWS, 512), bf16),
-        vmem((SIDE, ROWS, HALF), bf16), vmem((SIDE, ROWS, HALF), bf16),
-        vmem((2, SIDE, ROWS, CHUNK), bf16), vmem((2, SIDE, ROWS, CHUNK), bf16),
-        vmem((2, SIDE, ROWS, CHUNK), bf16), vmem((2, SIDE, ROWS, CHUNK), bf16),
+        vmem((SIDE, ROWS, COLS_Z), bf16), vmem((SIDE, ROWS, COLS_Y), bf16),
+    ]
+    scratch += [vmem((SIDE, ROWS, width), bf16) for axis, start, width in PIECES] * 2
+    scratch += [
         vmem((ROWS, WIDTH), bf16), vmem((ROWS, WIDTH), f32),
         vmem((N_SP * CAP, ROWS), bf16), vmem((ROWS, N_SP * CAP), bf16), vmem((ROWS, N_SP * CAP), bf16),
-        vmem((CHUNKS, N_SP, CAP, CHUNK), bf16), vmem((CHUNKS, N_SP, CAP, CHUNK), bf16),
+    ]
+    scratch += [vmem((N_SP, CAP, width), bf16) for axis, start, width in PIECES] * 2
+    scratch += [
         vmem((N_SP, CAP, WIDTH), bf16), vmem((N_SP, CAP, WIDTH), bf16),
-        vmem((N_SP * CAP, CHUNK), bf16), vmem((N_SP * CAP, HEAD), f32),
+        vmem((N_SP * CAP, 1024), bf16), vmem((N_SP * CAP, HEAD), f32),
         vmem((N_SP * CAP, FFE), f32), vmem((N_SP * CAP, FFE), f32),
         vmem((GROUP_ROWS, FFE), bf16),
         vmem((WIDTH, FFE), bf16), vmem((WIDTH, FFE), bf16), vmem((FFE, WIDTH), bf16),
         dma((6,)), dma((3,)), dma((3,)), dma((2,)), dma((2,)), dma((2,)), dma((2,)),
-        dma((2,)), dma((SIDE,)), dma, dma((2,)), dma((2,)), dma((2,)),
-        dma, dma((CHUNKS - 1 + GROUPS,)), dma, dma((GROUPS,)),
+        dma((2,)), dma((SIDE,)), dma, dma((4,)), dma((4,)),
+        dma((4,)), dma((EARLY,)), dma((2, GROUPS)), dma, dma((GROUPS,)),
     ]
     return pl.pallas_call(
         body_kernel,
-        out_shape=jax.ShapeDtypeStruct((1, ROWS, WIDTH), bf16),
+        out_shape=pltpu.VMEM((1, ROWS, WIDTH), bf16),
         in_specs=[anywhere] * 5 + [inside] * 3 + [anywhere] * 3,
         out_specs=inside,
         scratch_shapes=scratch,

time: 108 us -> 101 us (0.935)
  Pallas kernels: 105 us -> 99.7 us
    pallas_call x1, Pallas kernels: 105 us -> 99.7 us  [body(): pl.pallas_call(body_kernel, out_shape=pltpu.VMEM((1, ROWS, WIDTH), bf16),...]
    unnamed x1, local copies, waits for them, and re-layouts: 1.88 us -> 0.8 us
where the time goes in v5:
time: 101 us; the launch traced here: 100 us
  Pallas kernels  99.7 us (99%)
    pallas_call x1, Pallas kernels, body(): pl.pallas_call(body_kernel, out_shape=pltpu.VMEM((1, ROWS, WIDTH), bf16),...  99.7 us

profile of v5, /device:TPU:0, one launch (start us, length us, event | category | flops | bytes accessed | tf_op | source)
XLA Modules:
  0.0 100.5 jit_solution(6835284285449524912)
XLA Ops:
  0.0 99.7 %layer.1 = bf16[1,128,2048]{2,1,0:T(8,128)(2,1)S(1)} custom-call(bf16[1,128,2048]{2,1,0:T(8,128)(2,1)} %q_hbm.1, bf16[1,128,2048]{2,1,0:T(8,128)(2,1)} %k_hbm.1, bf16[1,128,2048]{2,1,0:T(8,128)(2,1)} %v_hbm.1, bf16[128,2048]{1,0:T(8,128)(2,1)} %proj_hbm.1, bf16[1,128,2048]{2,1,0:T(8,128)(2,1)} %res_hbm.1, f32[1,2048]{1,0:T(1,128)} %bitcast.3, ...), custom_call_target="tpu_custom_call" | custom-call | tf_op jit(solution)/shard_map/layer/pallas_call | solution.py:439
  99.7 0.8 copy.13

commit v6 on v5

--- a/solution.py
+++ b/solution.py
@@ -109,12 +109,6 @@
     for t in range(3):
         for a, b in others:
             send_heads(t, a, b)
-    for s in line:
-        remote(proj_hbm.at[core_rows, pl.ds(0, COLS_Z)], proj_a.at[y, core_rows],
-               proj_send.at[0], proj_recv.at[0], at(0, s))
-    for s in line:
-        remote(proj_hbm.at[core_rows, pl.ds(COLS_Z, COLS_Y)], proj_b.at[z, core_rows],
-               proj_send.at[1], proj_recv.at[1], at(s, 0))
     loads += [
         local(res_hbm.at[0], res, local_sem.at[0]),
         local(wg_hbm.at[0], wg, local_sem.at[1]),
@@ -155,6 +149,12 @@
     mix_lo[...] = (mix - high.astype(jnp.float32)).astype(jnp.bfloat16)
 
     wait_for(kh, head_recv.at[0])
+    for s in line:
+        remote(proj_hbm.at[core_rows, pl.ds(0, COLS_Z)], proj_a.at[y, core_rows],
+               proj_send.at[0], proj_recv.at[0], at(0, s))
+    for s in line:
+        remote(proj_hbm.at[core_rows, pl.ds(COLS_Z, COLS_Y)], proj_b.at[z, core_rows],
+               proj_send.at[1], proj_recv.at[1], at(s, 0))
     wait_for(qh, head_recv.at[1])
     scale = HEAD ** (-0.5)
 

time: 101 us -> 101 us (level)
  no operation moved by 1% of the time
where the time goes in v6:
time: 101 us; the launch traced here: 100 us
  Pallas kernels  99.6 us (99%)
    pallas_call x1, Pallas kernels, body(): pl.pallas_call(body_kernel, out_shape=pltpu.VMEM((1, ROWS, WIDTH), bf16),...  99.6 us

profile of v6, /device:TPU:0, one launch (start us, length us, event | category | flops | bytes accessed | tf_op | source)
XLA Modules:
  0.0 100.4 jit_solution(5243680465158231516)
XLA Ops:
  0.0 99.6 %layer.1 = bf16[1,128,2048]{2,1,0:T(8,128)(2,1)S(1)} custom-call(bf16[1,128,2048]{2,1,0:T(8,128)(2,1)} %q_hbm.1, bf16[1,128,2048]{2,1,0:T(8,128)(2,1)} %k_hbm.1, bf16[1,128,2048]{2,1,0:T(8,128)(2,1)} %v_hbm.1, bf16[128,2048]{1,0:T(8,128)(2,1)} %proj_hbm.1, bf16[1,128,2048]{2,1,0:T(8,128)(2,1)} %res_hbm.1, f32[1,2048]{1,0:T(1,128)} %bitcast.3, ...), custom_call_target="tpu_custom_call" | custom-call | tf_op jit(solution)/shard_map/layer/pallas_call | solution.py:439
  99.6 0.8 copy.13

commit v7 on v5

--- a/solution.py
+++ b/solution.py
@@ -64,7 +64,7 @@
         return ((z + a) % SIDE) * SIDE + (y + b) % SIDE
 
     others = [s for s in SHIFTS if s != (0, 0)]
-    line = (2, 1, 3)
+    line = (2, 3, 1)
 
     barrier = pltpu.get_barrier_semaphore()
     for a, b in others:

time: 101 us -> 101 us (level)
  no operation moved by 1% of the time
where the time goes in v7:
time: 101 us; the launch traced here: 100 us
  Pallas kernels  99.7 us (99%)
    pallas_call x1, Pallas kernels, body(): pl.pallas_call(body_kernel, out_shape=pltpu.VMEM((1, ROWS, WIDTH), bf16),...  99.7 us

profile of v7, /device:TPU:0, one launch (start us, length us, event | category | flops | bytes accessed | tf_op | source)
XLA Modules:
  0.0 100.5 jit_solution(10121791407936512743)
XLA Ops:
  0.0 99.7 %layer.1 = bf16[1,128,2048]{2,1,0:T(8,128)(2,1)S(1)} custom-call(bf16[1,128,2048]{2,1,0:T(8,128)(2,1)} %q_hbm.1, bf16[1,128,2048]{2,1,0:T(8,128)(2,1)} %k_hbm.1, bf16[1,128,2048]{2,1,0:T(8,128)(2,1)} %v_hbm.1, bf16[128,2048]{1,0:T(8,128)(2,1)} %proj_hbm.1, bf16[1,128,2048]{2,1,0:T(8,128)(2,1)} %res_hbm.1, f32[1,2048]{1,0:T(1,128)} %bitcast.3, ...), custom_call_target="tpu_custom_call" | custom-call | tf_op jit(solution)/shard_map/layer/pallas_call | solution.py:439
  99.7 0.8 copy.13
